TPU v7x, 256 devices: a whole 4x4x8 slice. The times are simulated.
256 devices in a mesh: sp: 64 (over z, x, core), tp: 4 (over y).
Axes of the slice: x: 4, y: 4, z: 8, core: 2. Of those that a mesh axis runs over, the one named last changes fastest.
Arguments:
- query_nope: bfloat16 [16384, 1024], P('sp', 'tp'), may hold values from -24 to 24
- query_rope: bfloat16 [16384, 512], P('sp', 'tp'), may hold values from -384 to 384
- latent: bfloat16 [16384, 256], P('sp'), may hold values from -6 to 6
- key_rope: bfloat16 [16384, 64], P('sp'), may hold values from -8 to 8
- latent_gain: bfloat16 [256], replicated, may hold values from 0.099609375 to 1.8984375
- key_up: bfloat16 [256, 1024], replicated, may hold values from -0.375 to 0.375
- value_up: bfloat16 [256, 1024], replicated, may hold values from -0.375 to 0.375
- out_proj: bfloat16 [1024, 2048], P('tp'), may hold values from -0.1875 to 0.1875
- residual: bfloat16 [16384, 2048], P(('sp', 'tp')), may hold values from -6 to 6
- ffn_gain: bfloat16 [2048], replicated, may hold values from 0.099609375 to 1.8984375
- expert_ids: int32 [16384, 4], P(('sp', 'tp')), may hold values from 0 to 63, all different within a row; in each aligned block of 64 rows (0 to 63, 64 to 127, ...) at most 8 rows name the same one
- route_weights: float32 [16384, 4], P(('sp', 'tp')), may hold values from 0.1 to 1
- expert_gate: bfloat16 [64, 2048, 384], P('sp'), may hold values from -0.125 to 0.125
- expert_up: bfloat16 [64, 2048, 384], P('sp'), may hold values from -0.125 to 0.125
- expert_down: bfloat16 [64, 384, 2048], P('sp'), may hold values from -0.3125 to 0.3125
- shared_gate: bfloat16 [2048, 384], replicated, may hold values from -0.125 to 0.125
- shared_up: bfloat16 [2048, 384], replicated, may hold values from -0.125 to 0.125
- shared_down: bfloat16 [384, 2048], replicated, may hold values from -0.3125 to 0.3125
Outputs:
- layer_out: bfloat16 [16384, 2048], P(('sp', 'tp'))
Inputs may be any that keep to these rules, and one draw needn't show every extreme that they name: `expert_ids`: each row names 4 different experts; among the 64 rows of one aligned block no expert is named by more than 8 rows.
All inputs are finite; a program needn't handle non-finite values.
Results may differ from a plain program's by a relative error of at most 0.017.
Values may be sent and summed in bfloat16 or wider, within the bound.
A program may use at most 128 MiB of HBM per device.

v0:
```python
import math

import jax
import jax.numpy as jnp
from jax import lax
from jax.sharding import PartitionSpec as P

NOPE = 128
ROPE = 64
VDIM = 128


rope_base = 10000.0
norm_eps = 1e-06


def sent_together(arrays, axis, dim, along):
    both = jnp.concatenate(arrays, axis=along)
    whole, at, done = (lax.all_gather(both, axis, axis=dim, tiled=True), 0, [])
    for a in arrays:
        done.append(lax.slice_in_dim(whole, at, at + a.shape[along], axis=along))
        at += a.shape[along]
    return tuple(done)


def split_up(shard, dim, size):
    before, after = (shard.shape[:dim], shard.shape[dim + 1 :])
    return jnp.moveaxis(shard.reshape(*before, size, -1, *after), dim, 0)


def sent_and_summed(shard, axis, dim):
    size = lax.axis_size(axis)
    pieces = lax.all_to_all(split_up(shard, dim, size), axis, 0, 0, tiled=True)
    return jnp.sum(pieces.astype(jnp.float32), axis=0)


def scale_rows(values, gain_vec):
    as_float = values.astype(jnp.float32)
    factor = lax.rsqrt(jnp.mean(as_float * as_float, axis=-1, keepdims=True) + norm_eps)
    return (as_float * factor * gain_vec.astype(jnp.float32)).astype(jnp.bfloat16)


def rotate(values, positions):
    half_dim = values.shape[-1] // 2
    frequency = rope_base ** (-jnp.arange(half_dim, dtype=jnp.float32) / half_dim)
    angles = positions.astype(jnp.float32)[:, None, None] * frequency
    cosine = jnp.cos(angles)
    sine_part = jnp.sin(angles)
    as_float = values.astype(jnp.float32)
    first_half = as_float[..., :half_dim]
    second_half = as_float[..., half_dim:]
    return jnp.concatenate(
        [
            first_half * cosine - second_half * sine_part,
            first_half * sine_part + second_half * cosine,
        ],
        axis=-1,
    ).astype(jnp.bfloat16)


def body(
    query_nope,
    query_rope,
    latent,
    key_rope,
    latent_gain,
    key_up,
    value_up,
    out_proj,
    residual,
    ffn_gain,
    expert_ids,
    route_weights,
    expert_gate,
    expert_up,
    expert_down,
    shared_gate,
    shared_up,
    shared_down,
):
    row_count = latent.shape[0]
    first_row = lax.axis_index("sp") * row_count
    last_row = first_row + row_count - 1
    positions = first_row + jnp.arange(row_count, dtype=jnp.int32)
    local_heads = query_nope.shape[1] // NOPE
    head_start = lax.axis_index("tp") * local_heads
    key_local = lax.dynamic_slice_in_dim(key_up, head_start * NOPE, local_heads * NOPE, 1)
    value_local = lax.dynamic_slice_in_dim(value_up, head_start * VDIM, local_heads * VDIM, 1)
    normed_latent = scale_rows(latent, latent_gain)
    rot_key = rotate(key_rope[:, None, :], positions)[:, 0, :]
    queries_nope = query_nope.reshape(row_count, local_heads, NOPE)
    rot_query = rotate(query_rope.reshape(row_count, local_heads, ROPE), positions)
    score_scale = 1.0 / math.sqrt(NOPE + ROPE)

    def attend(state_now, keys_flat, values_flat, keys_rope, key_start):
        running, weight_sum, weighted = state_now
        key_count = keys_flat.shape[0]
        key_heads = keys_flat.reshape(key_count, local_heads, NOPE)
        value_heads = values_flat.reshape(key_count, local_heads, VDIM)
        scores = jnp.einsum(
            "qhd,khd->hqk", queries_nope, key_heads, preferred_element_type=jnp.float32
        )
        scores = (
            scores
            + jnp.einsum("qhd,kd->hqk", rot_query, keys_rope, preferred_element_type=jnp.float32)
        ) * score_scale
        key_pos = key_start + jnp.arange(key_count, dtype=jnp.int32)
        allowed = (key_pos[None, :] <= positions[:, None])[None]
        scores = jnp.where(allowed, scores, -1e30)
        newest = jnp.maximum(running, jnp.max(scores, axis=-1))
        weights = jnp.where(allowed, jnp.exp(scores - newest[..., None]), 0.0)
        shrink = jnp.exp(running - newest)
        weight_sum = weight_sum * shrink + jnp.sum(weights, axis=-1)
        mixed = jnp.einsum(
            "hqk,khd->qhd",
            weights.astype(jnp.bfloat16),
            value_heads,
            preferred_element_type=jnp.float32,
        )
        weighted = weighted * shrink.T[:, :, None] + mixed
        return (newest, weight_sum, weighted)

    initial = (
        jnp.full((local_heads, row_count), -jnp.inf, jnp.float32),
        jnp.zeros((local_heads, row_count), jnp.float32),
        jnp.zeros((row_count, local_heads, VDIM), jnp.float32),
    )
    keys_flat = jnp.dot(normed_latent, key_local, preferred_element_type=jnp.float32).astype(
        jnp.bfloat16
    )
    values_flat = jnp.dot(normed_latent, value_local, preferred_element_type=jnp.float32).astype(
        jnp.bfloat16
    )
    pieces = sent_together((keys_flat, values_flat, rot_key), "sp", 0, 1)
    piece_len = pieces[0].shape[0]
    span_len = math.gcd(piece_len, 1024)

    def advance(step_num, state_in):
        offset = step_num * span_len
        sliced = tuple((lax.dynamic_slice_in_dim(member, offset, span_len, 0) for member in pieces))

        def compute(state_cur):
            keys_flat, values_flat = (sliced[0], sliced[1])
            return attend(state_cur, keys_flat, values_flat, sliced[-1], offset)

        def unchanged(state_cur):
            return state_cur

        return lax.cond(offset <= last_row, compute, unchanged, state_in)

    folded = lax.fori_loop(0, piece_len // span_len, advance, initial)
    heads_out = (
        (folded[2] / folded[1].T[:, :, None])
        .astype(jnp.bfloat16)
        .reshape(row_count, local_heads * VDIM)
    )
    tokens = residual.shape[0]
    attn_sum = sent_and_summed(
        jnp.dot(heads_out, out_proj, preferred_element_type=jnp.float32).astype(jnp.bfloat16),
        "tp",
        0,
    )
    hidden_one = (residual.astype(jnp.float32) + attn_sum).astype(jnp.bfloat16)
    normed = scale_rows(hidden_one, ffn_gain)
    slot_count = expert_ids.shape[1]
    model_width = residual.shape[1]
    local_experts = expert_gate.shape[0]
    experts = local_experts * lax.axis_size("sp")
    capacity = max(2, 2 * tokens * slot_count // experts)
    flat_ids = expert_ids.reshape(-1)
    onehot = (flat_ids[:, None] == jnp.arange(experts, dtype=jnp.int32)[None, :]).astype(jnp.int32)
    slot_rank = jnp.sum(jnp.cumsum(onehot, axis=0) * onehot, axis=1) - 1
    target = flat_ids * capacity + slot_rank
    slot_token = (
        jnp.full((experts * capacity,), tokens, jnp.int32)
        .at[target]
        .set(jnp.arange(tokens * slot_count, dtype=jnp.int32) // slot_count)
    )
    padded = jnp.concatenate([normed, jnp.zeros((1, model_width), jnp.bfloat16)], axis=0)
    outgoing = padded[slot_token].reshape(experts, capacity, model_width)
    arrived = lax.all_to_all(outgoing, "sp", split_axis=0, concat_axis=0, tiled=True)
    item_count = arrived.shape[1]
    grouped = arrived.reshape(-1, local_experts, item_count, model_width)
    gate_part = jnp.einsum(
        "seid,edf->seif", grouped, expert_gate, preferred_element_type=jnp.float32
    )
    upper_part = jnp.einsum(
        "seid,edf->seif", grouped, expert_up, preferred_element_type=jnp.float32
    )
    expert_hidden = (jax.nn.silu(gate_part) * upper_part).astype(jnp.bfloat16)
    expert_rows = jnp.einsum(
        "seif,efd->seid", expert_hidden, expert_down, preferred_element_type=jnp.float32
    ).astype(jnp.bfloat16)
    answered = expert_rows.reshape(-1, item_count, model_width)
    returned = lax.all_to_all(answered, "sp", split_axis=0, concat_axis=0, tiled=True)
    picked = returned.reshape(experts * capacity, model_width)[target]
    routed = jnp.sum(
        (picked.astype(jnp.float32) * route_weights.reshape(-1)[:, None]).reshape(
            tokens, slot_count, model_width
        ),
        axis=1,
    ).astype(jnp.bfloat16)
    shared_gate_part = jnp.dot(normed, shared_gate, preferred_element_type=jnp.float32)
    shared_upper = jnp.dot(normed, shared_up, preferred_element_type=jnp.float32)
    shared_hidden = (jax.nn.silu(shared_gate_part) * shared_upper).astype(jnp.bfloat16)
    shared_rows = jnp.dot(shared_hidden, shared_down, preferred_element_type=jnp.float32).astype(
        jnp.bfloat16
    )
    return (
        hidden_one.astype(jnp.float32)
        + routed.astype(jnp.float32)
        + shared_rows.astype(jnp.float32)
    ).astype(jnp.bfloat16)


def solution(mesh):
    in_specs = (
        P("sp", "tp"),
        P("sp", "tp"),
        P("sp", None),
        P("sp", None),
        P(),
        P(),
        P(),
        P("tp", None),
        P(("sp", "tp"), None),
        P(),
        P(("sp", "tp"), None),
        P(("sp", "tp"), None),
        P("sp", None, None),
        P("sp", None, None),
        P("sp", None, None),
        P(),
        P(),
        P(),
    )
    out_specs = P(("sp", "tp"), None)
    return jax.shard_map(body, mesh=mesh, in_specs=in_specs, out_specs=out_specs, check_vma=False)
```

profile of v0, /device:TPU:1, one launch (start us, length us, event | category | flops | bytes accessed | tf_op | source)
XLA Modules:
  0.0 386.5 jit_solution(3514274997987511048)
XLA Ops:
  6.6 1.1 fusion.51
  7.8 0.7 convert_element_type.119
  8.4 1.3 convolution_convert_fusion.3
  9.7 1.3 convolution_convert_fusion.4
  11.0 0.8 bitcast_convert_fusion
  11.9 0.8 pad_maximum_fusion
  12.7 0.8 copy.32
  14.1 0.6 reduce-window.6
  15.3 113.3 %all-gather.2.cloned.1.call-done = bf16[16384,576]{0,1:T(8,128)(2,1)} async-done(((bf16[256,576]{0,1:T(8,128)(2,1)}), bf16[16384,576]{0,1:T(8,128)(2,1)}) %all-gather.2.cloned.1.call-update) | async-done | bytes 18874384 | tf_op jit(solution)/shard_map/all_gather | solution.py:19
  128.6 11.6 %fusion.88 = (bf16[16384,256]{0,1:T(8,128)(2,1)}, bf16[16384,256]{0,1:T(8,128)(2,1)}) fusion(bf16[16384,576]{0,1:T(8,128)(2,1)} %all-gather.2.cloned.1.call-done), kind=kLoop, calls=%fused_computation.125 | loop fusion | bytes 33554432 | tf_op jit(solution)/shard_map/slice | solution.py:21
  140.2 3.1 slice.43
  143.4 5.8 %while.18 = (s32[]{:T(128)}, f32[2,256]{1,0:T(2,128)S(1)}, f32[2,256]{1,0:T(2,128)S(1)}, f32[256,2,128]{2,0,1:T(8,128)S(1)}, s32[]{:T(128)}, /*index=5*/bf16[163...) while((s32[]{:T(128)}, f32[2,256]{1,0:T(2,128)S(1)}, ...), condition=%wide.region_6.7_spmd.clone, body=%wide.region_1.6_spmd.clone.sunk | while | flops 341183232 | bytes 15577433 | solution.py:151
  143.4 4.9 %conditional.3 = ((f32[2,256]{1,0:T(2,128)S(1)}, f32[2,256]{1,0:T(2,128)S(1)}, f32[256,2,128]{2,0,1:T(8,128)S(1)})) conditional(s32[]{:T(128)} %convert_element_type.219, (f32[2,256]{1,0:T(2,128)S(1)}, f32[2,256]{1,0:T(2,128)S(1)}, f32[256,2,128]{2,0,1:T(8,128)S(1)}) %tuple.61, (s32[]{:T(128)}, s32[]{:T(128)}, bf16[16384,256]{0,1:T(8,128)(2,1)}, ...), branch_computations={%region_2.0_spmd, %region_3.5_spmd} | conditional | flops 341183232 | bytes 15576146 | solution.py:149
  143.4 1.4 constant_dynamic-slice_fusion
  145.5 1.5 fusion.87
  147.0 0.8 fusion.6
  149.3 1.5 convolution_convert_fusion.1
  150.8 4.1 %all-to-all-start = ((bf16[4,64,2048]{2,1,0:T(8,128)(2,1)}), bf16[4,64,2048]{2,1,0:T(8,128)(2,1)S(1)}, u32[]{:S(2)}, u32[]{:S(2)}) async-start(bf16[4,64,2048]{2,1,0:T(8,128)(2,1)} %bitcast.114), calls=%async_computation | async-start | bytes 2097152 | tf_op jit(solution)/shard_map/all_to_all | solution.py:33
  155.1 1.4 scatter_custom_fusion
  156.6 13.0 %all-to-all-done = bf16[4,64,2048]{2,1,0:T(8,128)(2,1)S(1)} async-done(((bf16[4,64,2048]{2,1,0:T(8,128)(2,1)}), bf16[4,64,2048]{2,1,0:T(8,128)(2,1)S(1)}, u32[]{:S(2)}, u32[]{:S(2)}) %all-to-all-start) | async-done | bytes 1048608 | tf_op jit(solution)/shard_map/all_to_all | solution.py:33
  170.1 3.3 gather_fusion
  173.4 128.1 %all_to_all.15 = bf16[64,8,2048]{2,1,0:T(8,128)(2,1)S(1)} all-to-all(bf16[64,8,2048]{2,1,0:T(8,128)(2,1)} %bitcast.113), channel_id=1, replica_groups=mesh['sp'=64,'tp'=4] {'sp'}, dimensions={0} | all-to-all | bytes 4194304 | tf_op jit(solution)/shard_map/all_to_all | solution.py:181
  301.5 1.3 copy-done.1
  302.8 1.2 fusion.24
  304.1 5.7 %convolution_convert_fusion = bf16[64,8,2048]{2,1,0:T(8,128)(2,1)} fusion(bf16[1,384,2048]{2,1,0:T(8,128)(2,1)S(1)} %copy-done, bf16[64,8,2048]{2,1,0:T(8,128)(2,1)} %copy-done.1, bf16[1,2048,384]{2,1,0:T(8,128)(2,1)} %param.35, f32[64,1,8,384]{3,2,0,1:T(8,128)S(1)} %fusion.24), kind=kOutput, calls=%fused_computation.27 | convolution fusion | flops 1612840960 | bytes 8126464 | tf_op jit(solution)/shard_map/seif,efd->seid/dot_general | solution.py:191
  309.8 7.3 %all-to-all-start.2 = ((bf16[64,8,2048]{2,1,0:T(8,128)(2,1)}), bf16[64,8,2048]{2,1,0:T(8,128)(2,1)}, u32[]{:S(2)}, u32[]{:S(2)}) async-start(bf16[64,8,2048]{2,1,0:T(8,128)(2,1)} %convolution_convert_fusion), calls=%async_computation.2 | async-start | bytes 4194304 | tf_op jit(solution)/shard_map/all_to_all | solution.py:195
  317.3 1.8 fusion.85
  319.1 48.0 %all-to-all-done.2 = bf16[64,8,2048]{2,1,0:T(8,128)(2,1)} async-done(((bf16[64,8,2048]{2,1,0:T(8,128)(2,1)}), bf16[64,8,2048]{2,1,0:T(8,128)(2,1)}, u32[]{:S(2)}, u32[]{:S(2)}) %all-to-all-start.2) | async-done | bytes 2097184 | tf_op jit(solution)/shard_map/all_to_all | solution.py:195
  367.1 4.2 %gather_fusion.1 = bf16[256,2048]{1,0:T(8,128)(2,1)S(1)} fusion(bf16[512,2048]{1,0:T(8,128)(2,1)} %bitcast.35, s32[1024]{0:T(1024)S(1)} %pad_clamp_fusion), kind=kCustom, calls=%fused_computation.1 | custom fusion | bytes 2098176 | tf_op jit(solution)/shard_map/gather | solution.py:196
  371.3 1.7 reshape.307
  373.0 3.2 multiply_reduce_fusion
  376.2 3.4 fusion.18
  (98 shorter events, 3.8 us)
Async XLA Ops:
  6.5 297.5 %copy-start = (bf16[1,384,2048]{2,1,0:T(8,128)(2,1)S(1)}, bf16[1,384,2048]{2,1,0:T(8,128)(2,1)}, u32[]{:S(2)}) copy-start(bf16[1,384,2048]{2,1,0:T(8,128)(2,1)} %param.36) | copy-start | bytes 4718596
  6.5 8.7 %copy-start.6 = (s32[64,4]{0,1:T(4,128)S(1)}, s32[64,4]{0,1:T(4,128)}, u32[]{:S(2)}) copy-start(s32[64,4]{0,1:T(4,128)} %param.32) | copy-start | bytes 3076
  6.5 7.2 %copy-start.5 = (bf16[256,128]{1,0:T(8,128)(2,1)S(1)}, bf16[256,128]{1,0:T(8,128)(2,1)}, u32[]{:S(2)}) copy-start(bf16[256,128]{1,0:T(8,128)(2,1)} %param.23) | copy-start | bytes 196612
  6.5 7.3 %copy-start.4 = (bf16[256,256]{1,0:T(8,128)(2,1)S(1)}, bf16[256,256]{1,0:T(8,128)(2,1)}, u32[]{:S(2)}) copy-start(bf16[256,256]{1,0:T(8,128)(2,1)} %param.22) | copy-start | bytes 393220
  6.5 122.0 %all-gather.2.cloned.1.call-start = ((), (), s32[]{:S(2)}) async-start(), calls=%async_computation.3 | async-start | bytes 19169280 | tf_op jit(solution)/shard_map/all_gather | solution.py:19
  143.3 6.0 %copy-start.2 = (bf16[256,2048]{1,0:T(8,128)(2,1)S(1)}, bf16[256,2048]{1,0:T(8,128)(2,1)}, u32[]{:S(2)}) copy-start(bf16[256,2048]{1,0:T(8,128)(2,1)} %param.29) | copy-start | bytes 3145732
  149.3 5.6 %copy-start.7 = (bf16[2048]{0:T(1024)(128)(2,1)S(1)}, bf16[2048]{0:T(1024)(128)(2,1)}, u32[]{:S(2)}) copy-start(bf16[2048]{0:T(1024)(128)(2,1)} %param.31) | copy-start | bytes 12292
  150.8 18.9 %copy-start.3 = (bf16[64,2048]{1,0:T(8,128)(2,1)S(1)}, bf16[64,2048]{1,0:T(8,128)(2,1)}, u32[]{:S(2)}) copy-start(bf16[64,2048]{1,0:T(8,128)(2,1)} %param.30) | copy-start | bytes 786436
  150.8 18.8 %all-to-all-start = ((bf16[4,64,2048]{2,1,0:T(8,128)(2,1)}), bf16[4,64,2048]{2,1,0:T(8,128)(2,1)S(1)}, u32[]{:S(2)}, u32[]{:S(2)}) async-start(bf16[4,64,2048]{2,1,0:T(8,128)(2,1)} %bitcast.114), calls=%async_computation | async-start | bytes 2097152 | tf_op jit(solution)/shard_map/all_to_all | solution.py:33
  173.4 129.4 %copy-start.9 = (bf16[1,2048,384]{2,1,0:T(8,128)(2,1)S(1)}, bf16[1,2048,384]{2,1,0:T(8,128)(2,1)}, u32[]{:S(2)}) copy-start(bf16[1,2048,384]{2,1,0:T(8,128)(2,1)} %param.34) | copy-start | bytes 4718596
  301.5 1.3 copy-start.1
  309.8 7.3 %copy-start.8 = (f32[64,4]{0,1:T(4,128)S(1)}, f32[64,4]{0,1:T(4,128)}, u32[]{:S(2)}) copy-start(f32[64,4]{0,1:T(4,128)} %param.33) | copy-start | bytes 3076
  309.8 57.2 %all-to-all-start.2 = ((bf16[64,8,2048]{2,1,0:T(8,128)(2,1)}), bf16[64,8,2048]{2,1,0:T(8,128)(2,1)}, u32[]{:S(2)}, u32[]{:S(2)}) async-start(bf16[64,8,2048]{2,1,0:T(8,128)(2,1)} %convolution_convert_fusion), calls=%async_computation.2 | async-start | bytes 4194304 | tf_op jit(solution)/shard_map/all_to_all | solution.py:195
Sparse Core Ops, SparseCore 0:
  12.8 115.6 all-gather.1
where the time goes:
time: 388 us; the launch traced here: 386 us
  waiting for transfers between devices  174 us (45%)
  blocking collectives  128 us (33%)
  local copies, waits for them, and re-layouts  30.1 us (8%)
  matrix products  19 us (5%)
  between operations  13.7 us (4%)
  starting transfers between devices  11.5 us (3%)
  other arithmetic  8.91 us (2%)
    all_to_all x1, blocking collectives, body(): lax.all_to_all(outgoing, 'sp', split_axis=0, concat_axis=0, tiled=True)  128 us
    all_gather x1, waiting for transfers between devices, sent_together(): whole, at, done = (lax.all_gather(both, axis, axis=dim, tiled=True), 0, [])  113 us
    all_to_all x1, waiting for transfers between devices, body(): lax.all_to_all(answered, 'sp', split_axis=0, concat_axis=0, tiled=True)  48 us
    slice x2, local copies, waits for them, and re-layouts, sent_together(): done.append(lax.slice_in_dim(whole, at, at + a.shape[along], axis=along))  14.7 us
    all_to_all x1, waiting for transfers between devices, sent_and_summed(): pieces = lax.all_to_all(split_up(shard, dim, size), axis, 0, 0, tiled=True)  13 us
  transfers between devices with their start and end apart: 3, of which 3 were waited for; matrix products, arithmetic and copies ran while one was open for 2% of the time, Pallas kernels for 0%

commit v1 on v0

v1 whole, which is shorter than its diff:
```python
import math

import jax
import jax.numpy as jnp
from jax import lax
from jax.experimental import pallas as pl
from jax.experimental.pallas import tpu as pltpu
from jax.sharding import Mesh, PartitionSpec as P

NOPE = 128
ROPE = 64
VDIM = 128
NZ, NX, NC, NY = 8, 4, 2, 4
CAP = 8
ROWS = 256
QUART = 64
PACK = 80

rope_base = 10000.0
norm_eps = 1e-06


def scale_rows(values, gain_vec):
    as_float = values.astype(jnp.float32)
    factor = lax.rsqrt(jnp.mean(as_float * as_float, axis=-1, keepdims=True) + norm_eps)
    return (as_float * factor * gain_vec.astype(jnp.float32)).astype(jnp.bfloat16)


def rotate(values, positions):
    half_dim = values.shape[-1] // 2
    frequency = rope_base ** (-jnp.arange(half_dim, dtype=jnp.float32) / half_dim)
    angles = positions.astype(jnp.float32)[:, None, None] * frequency
    cosine = jnp.cos(angles)
    sine_part = jnp.sin(angles)
    as_float = values.astype(jnp.float32)
    first_half = as_float[..., :half_dim]
    second_half = as_float[..., half_dim:]
    return jnp.concatenate(
        [
            first_half * cosine - second_half * sine_part,
            first_half * sine_part + second_half * cosine,
        ],
        axis=-1,
    ).astype(jnp.bfloat16)


KB = 4
LOG2E = 1.4426950408889634


def attend_kernel(first, last, meta, q_ref, g_ref, ku_ref, vu_ref, *refs):
    if first:
        state_in = None
        outs = refs[:1] if last else refs[:3]
        m_ref, l_ref, acc_ref = refs[-3:]
    else:
        mi_ref, li_ref, ai_ref = refs[:3]
        outs = refs[3:4] if last else refs[3:6]
        m_ref, l_ref, acc_ref = refs[-3:]
    i = pl.program_id(0)
    nsteps = pl.num_programs(0)
    q_sp = meta[0]
    core = meta[1]
    needed = meta[2]
    whole = meta[3]
    scale = LOG2E / math.sqrt(NOPE + ROPE)

    @pl.when(i == 0)
    def _():
        if first:
            m_ref[...] = jnp.full(m_ref.shape, -1e30, jnp.float32)
            l_ref[...] = jnp.zeros(l_ref.shape, jnp.float32)
            acc_ref[...] = jnp.zeros(acc_ref.shape, jnp.float32)
        else:
            m_ref[...] = mi_ref[...]
            l_ref[...] = li_ref[...]
            acc_ref[...] = ai_ref[...]

    def step(masked):
        keys = KB * ROWS
        lat = jnp.concatenate(
            [g_ref[b, y, 0:QUART, :] for b in range(KB) for y in range(NY)], axis=0
        )
        rope = jnp.concatenate(
            [
                g_ref[b, y, QUART:PACK, g * ROPE : (g + 1) * ROPE]
                for b in range(KB)
                for y in range(NY)
                for g in range(4)
            ],
            axis=0,
        )
        rope = jnp.concatenate([rope, jnp.zeros((keys, ROPE), jnp.bfloat16)], axis=1)
        k = jnp.dot(lat, ku_ref[...], preferred_element_type=jnp.float32).astype(jnp.bfloat16)
        v = jnp.dot(lat, vu_ref[...], preferred_element_type=jnp.float32).astype(jnp.bfloat16)
        if masked:
            j = lax.broadcasted_iota(jnp.int32, (1, keys), 1)
            chunk = i * KB + j // ROWS
            kpos = (chunk * 2 + core) * ROWS + j % ROWS
            qpos = q_sp * ROWS + lax.broadcasted_iota(jnp.int32, (ROWS, 1), 0)
            allowed = kpos <= qpos
        for h in range(2):
            kcat = jnp.concatenate([k[:, h * NOPE : (h + 1) * NOPE], rope], axis=1)
            s = lax.dot_general(
                q_ref[h], kcat, (((1,), (1,)), ((), ())), preferred_element_type=jnp.float32
            )
            s = s * scale
            if masked:
                s = jnp.where(allowed, s, -1e30)
            m_old = m_ref[h]
            m_new = jnp.maximum(m_old, jnp.max(s, axis=1, keepdims=True))
            p = jnp.exp2(s - m_new[:, :1])
            if masked:
                p = jnp.where(allowed, p, 0.0)
            alpha = jnp.exp2(m_old - m_new)
            l_ref[h] = l_ref[h] * alpha + jnp.sum(p, axis=1, keepdims=True)
            acc_ref[h] = acc_ref[h] * alpha + jnp.dot(
                p.astype(jnp.bfloat16),
                v[:, h * VDIM : (h + 1) * VDIM],
                preferred_element_type=jnp.float32,
            )
            m_ref[h] = m_new

    @pl.when(i < whole)
    def _():
        step(False)

    @pl.when((i >= whole) & (i < needed))
    def _():
        step(True)

    @pl.when(i == nsteps - 1)
    def _():
        if last:
            for h in range(2):
                outs[0][:, h * VDIM : (h + 1) * VDIM] = (acc_ref[h] / l_ref[h]).astype(jnp.bfloat16)
        else:
            outs[0][...] = m_ref[...]
            outs[1][...] = l_ref[...]
            outs[2][...] = acc_ref[...]


def attend(q_cat, gathered, key_local, value_local, q_sp, core, state):
    first = state is None
    last = not first
    have = jnp.maximum((q_sp - core) // 2 + 1, 0)
    have = jnp.where(q_sp < core, 0, have)
    needed = (have + KB - 1) // KB
    full = jnp.where(q_sp <= core, 0, (q_sp - core + 1) // 2)
    whole = full // KB
    meta = jnp.stack([q_sp, core, needed, whole]).astype(jnp.int32)
    nsteps = (NZ * NX) // KB
    state_spec = pl.BlockSpec((2, ROWS, 128), lambda i, meta: (0, 0, 0))
    in_specs = [
        pl.BlockSpec((2, ROWS, 256), lambda i, meta: (0, 0, 0)),
        pl.BlockSpec(
            (KB, NY, PACK, 256),
            lambda i, meta: (jnp.minimum(i, jnp.maximum(meta[2] - 1, 0)), 0, 0, 0),
        ),
        pl.BlockSpec((256, 256), lambda i, meta: (0, 0)),
        pl.BlockSpec((256, 256), lambda i, meta: (0, 0)),
    ]
    args = [q_cat, gathered, key_local, value_local]
    if not first:
        in_specs += [state_spec] * 3
        args += list(state)
    if last:
        out_shape = jax.ShapeDtypeStruct((ROWS, 256), jnp.bfloat16)
        out_specs = pl.BlockSpec((ROWS, 256), lambda i, meta: (0, 0))
    else:
        out_shape = tuple(jax.ShapeDtypeStruct((2, ROWS, 128), jnp.float32) for _ in range(3))
        out_specs = (state_spec,) * 3
    import functools

    return pl.pallas_call(
        functools.partial(attend_kernel, first, last),
        out_shape=out_shape,
        grid_spec=pltpu.PrefetchScalarGridSpec(
            num_scalar_prefetch=1,
            grid=(nsteps,),
            in_specs=in_specs,
            out_specs=out_specs,
            scratch_shapes=[pltpu.VMEM((2, ROWS, 128), jnp.float32)] * 3,
        ),
        compiler_params=pltpu.CompilerParams(dimension_semantics=("arbitrary",)),
        cost_estimate=pl.CostEstimate(
            flops=3_000_000_000, bytes_accessed=6_000_000, transcendentals=4_000_000
        ),
    )(meta, *args)


def body(
    query_nope,
    query_rope,
    latent,
    key_rope,
    latent_gain,
    key_up,
    value_up,
    out_proj,
    residual,
    ffn_gain,
    expert_ids,
    route_weights,
    expert_gate,
    expert_up,
    expert_down,
    shared_gate,
    shared_up,
    shared_down,
):
    z, x, core, y = (lax.axis_index(n) for n in ("z", "x", "core", "y"))
    q_sp = (z * NX + x) * NC + core
    first_row = q_sp * ROWS
    positions = first_row + jnp.arange(ROWS, dtype=jnp.int32)

    lat_q = lax.dynamic_slice_in_dim(latent, y * QUART, QUART, 0)
    rope_q = lax.dynamic_slice_in_dim(key_rope, y * QUART, QUART, 0)
    pos_q = first_row + y * QUART + jnp.arange(QUART, dtype=jnp.int32)
    normed_latent = scale_rows(lat_q, latent_gain)
    rot_key = rotate(rope_q[:, None, :], pos_q)[:, 0, :]
    packed_rope = jnp.concatenate([rot_key[g * 16 : (g + 1) * 16] for g in range(4)], axis=1)
    payload = jnp.concatenate([normed_latent, packed_rope], axis=0)
    mine = lax.all_gather(payload, ("z", "x", "y"), axis=0, tiled=False)
    mine = mine.reshape(NZ * NX, NY, PACK, 256)
    theirs = lax.ppermute(mine, "core", [(0, 1), (1, 0)])

    key_local = lax.dynamic_slice_in_dim(key_up, y * 256, 256, 1)
    value_local = lax.dynamic_slice_in_dim(value_up, y * 256, 256, 1)
    rot_query = rotate(query_rope.reshape(ROWS, 2, ROPE), positions)
    q_cat = jnp.concatenate(
        [
            query_nope.reshape(ROWS, 2, NOPE),
            rot_query,
            jnp.zeros((ROWS, 2, 64), jnp.bfloat16),
        ],
        axis=-1,
    ).transpose(1, 0, 2)

    flat_ids = expert_ids.reshape(-1)
    onehot = (flat_ids[:, None] == jnp.arange(64, dtype=jnp.int32)[None, :]).astype(jnp.float32)
    earlier = (
        jnp.arange(256, dtype=jnp.int32)[None, :] < jnp.arange(256, dtype=jnp.int32)[:, None]
    ).astype(jnp.float32)
    before = jnp.dot(earlier, onehot)
    rank = jnp.sum(before * onehot, axis=1).reshape(64, 4)
    tables = jnp.concatenate([expert_ids.astype(jnp.float32) * CAP + rank, route_weights], axis=1)
    tables = lax.all_gather(tables, "z", axis=0, tiled=False)
    slot_of = tables[:, :, :4] - (z * 64).astype(jnp.float32)
    weight_of = tables[:, :, 4:]
    slots = jnp.arange(64, dtype=jnp.float32)
    hit = slot_of[:, :, :, None] == slots
    pick = jnp.any(hit, axis=2).astype(jnp.bfloat16)
    share = jnp.sum(jnp.where(hit, weight_of[:, :, :, None], 0.0), axis=2)
    share_hi = share.astype(jnp.bfloat16)
    share_lo = (share - share_hi.astype(jnp.float32)).astype(jnp.bfloat16)

    state = attend(q_cat, mine, key_local, value_local, q_sp, core, None)
    heads_out = attend(q_cat, theirs, key_local, value_local, q_sp, 1 - core, state)

    part = jnp.dot(heads_out, out_proj, preferred_element_type=jnp.float32).astype(jnp.bfloat16)
    pieces = lax.all_to_all(part.reshape(4, 64, 2048), "y", 0, 0, tiled=True)
    attn_sum = jnp.sum(pieces.astype(jnp.float32), axis=0)
    hidden_one = (residual.astype(jnp.float32) + attn_sum).astype(jnp.bfloat16)
    normed = scale_rows(hidden_one, ffn_gain)

    column = lax.all_gather(normed, "z", axis=0, tiled=False)
    outgoing = jnp.einsum(
        "stk,std->skd", pick, column, preferred_element_type=jnp.float32
    ).astype(jnp.bfloat16)
    outgoing = outgoing.reshape(8, 8, CAP, 2048).transpose(1, 0, 2, 3)
    arrived = lax.all_to_all(outgoing, ("x", "core"), split_axis=0, concat_axis=0, tiled=True)
    grouped = arrived.reshape(512, 2048)
    gate_part = jnp.dot(grouped, expert_gate[0], preferred_element_type=jnp.float32)
    upper_part = jnp.dot(grouped, expert_up[0], preferred_element_type=jnp.float32)
    expert_hidden = (jax.nn.silu(gate_part) * upper_part).astype(jnp.bfloat16)
    expert_rows = jnp.dot(
        expert_hidden, expert_down[0], preferred_element_type=jnp.float32
    ).astype(jnp.bfloat16)
    returned = lax.all_to_all(
        expert_rows.reshape(8, 8, CAP, 2048), ("x", "core"), split_axis=0, concat_axis=0, tiled=True
    )
    back = returned.transpose(1, 0, 2, 3).reshape(8, 64, 2048)
    partial = jnp.einsum("stk,skd->std", share_hi, back, preferred_element_type=jnp.float32)
    partial = partial + jnp.einsum(
        "stk,skd->std", share_lo, back, preferred_element_type=jnp.float32
    )
    routed = lax.psum_scatter(
        partial.astype(jnp.bfloat16), "z", scatter_dimension=0, tiled=False
    )

    shared_gate_part = jnp.dot(normed, shared_gate, preferred_element_type=jnp.float32)
    shared_upper = jnp.dot(normed, shared_up, preferred_element_type=jnp.float32)
    shared_hidden = (jax.nn.silu(shared_gate_part) * shared_upper).astype(jnp.bfloat16)
    shared_rows = jnp.dot(shared_hidden, shared_down, preferred_element_type=jnp.float32).astype(
        jnp.bfloat16
    )
    return (
        hidden_one.astype(jnp.float32)
        + routed.astype(jnp.float32)
        + shared_rows.astype(jnp.float32)
    ).astype(jnp.bfloat16)


def solution(mesh):
    fine = Mesh(mesh.devices.reshape(NZ, NX, NC, NY), ("z", "x", "core", "y"))
    sp = ("z", "x", "core")
    every = ("z", "x", "core", "y")
    in_specs = (
        P(sp, "y"),
        P(sp, "y"),
        P(sp, None),
        P(sp, None),
        P(),
        P(),
        P(),
        P("y", None),
        P(every, None),
        P(),
        P(every, None),
        P(every, None),
        P(sp, None, None),
        P(sp, None, None),
        P(sp, None, None),
        P(),
        P(),
        P(),
    )
    return jax.shard_map(
        body, mesh=fine, in_specs=in_specs, out_specs=P(every, None), check_vma=False
    )
```

time: 388 us -> 363 us (0.936)
  blocking collectives: 128 us -> 77.1 us
  waiting for transfers between devices: 174 us -> 205 us
  local copies, waits for them, and re-layouts: 30.1 us -> 6.38 us
  Pallas kernels: 0 us -> 10.4 us
    all_to_all x1, blocking collectives: 128 us -> 35.3 us  [body(): lax.all_to_all(outgoing, ('x', 'core'), split_axis=0, concat_axis=0, tile...]
    all_gather x0 -> x1, blocking collectives: none -> 41.8 us  [body(): tables = lax.all_gather(tables, 'z', axis=0, tiled=False)]
    reduce_scatter x0 -> x1, waiting for transfers between devices: none -> 33.5 us  [body(): lax.psum_scatter(partial.astype(jnp.bfloat16), 'z', scatter_dimension=0,...]
    all_to_all x2, waiting for transfers between devices: 61 us -> 39.9 us  [the longest x1 25.7 us: body(): lax.all_to_all(expert_rows.reshape(8, 8, CAP, 2048), ('x', 'core'), split...]
    all_gather x1 -> x2, waiting for transfers between devices: 113 us -> 132 us  [the longest x1 118 us: body(): mine = lax.all_gather(payload, ('z', 'x', 'y'), axis=0, tiled=False)]
    slice x3 -> x5, local copies, waits for them, and re-layouts: 14.9 us -> 0.33 us  [the longest x4 0.32 us: body(): rot_key[g * 16:(g + 1) * 16]]
    pallas_call x0 -> x2, Pallas kernels: none -> 10.4 us  [attend(): pl.pallas_call(functools.partial(attend_kernel, first, last), out_shape=o...]
    gather x2 -> x0, local copies, waits for them, and re-layouts: 7.57 us -> none  [the longest x1 4.22 us: body(): picked = returned.reshape(experts * capacity, model_width)[target]]
  transfers between devices with their start and end apart: 3 -> 6, of which waited for: 3 -> 5; matrix products, arithmetic and copies ran while one was open for 2% -> 3% of each run, Pallas kernels for 0% -> 1%
where the time goes in v1:
time: 363 us; the launch traced here: 358 us
  waiting for transfers between devices  205 us (56%)
  blocking collectives  77.1 us (21%)
  matrix products  22.7 us (6%)
  starting transfers between devices  13.7 us (4%)
  between operations  13.4 us (4%)
  Pallas kernels  10.4 us (3%)
  other arithmetic  9.16 us (3%)
  local copies, waits for them, and re-layouts  6.38 us (2%)
    all_gather x1, waiting for transfers between devices, body(): mine = lax.all_gather(payload, ('z', 'x', 'y'), axis=0, tiled=False)  118 us
    all_gather x1, blocking collectives, body(): tables = lax.all_gather(tables, 'z', axis=0, tiled=False)  41.8 us
    all_to_all x1, blocking collectives, body(): lax.all_to_all(outgoing, ('x', 'core'), split_axis=0, concat_axis=0, tile...  35.3 us
    reduce_scatter x1, waiting for transfers between devices, body(): lax.psum_scatter(partial.astype(jnp.bfloat16), 'z', scatter_dimension=0,...  33.5 us
    all_to_all x1, waiting for transfers between devices, body(): lax.all_to_all(expert_rows.reshape(8, 8, CAP, 2048), ('x', 'core'), split...  25.7 us
    all_to_all x1, waiting for transfers between devices, body(): pieces = lax.all_to_all(part.reshape(4, 64, 2048), 'y', 0, 0, tiled=True)  14.2 us
    all_gather x1, waiting for transfers between devices, body(): column = lax.all_gather(normed, 'z', axis=0, tiled=False)  13.4 us
    pallas_call x2, Pallas kernels, attend(): pl.pallas_call(functools.partial(attend_kernel, first, last), out_shape=o...  10.4 us
  transfers between devices with their start and end apart: 6, of which 5 were waited for; matrix products, arithmetic and copies ran while one was open for 3% of the time, Pallas kernels for 1%

profile of v1, /device:TPU:1, one launch (start us, length us, event | category | flops | bytes accessed | tf_op | source)
XLA Modules:
  0.0 358.1 jit_solution(14747740260441493155)
XLA Ops:
  6.6 0.9 bitcast_convert_fusion
  8.0 0.7 convert_element_type.120
  8.7 0.9 fusion.39
  9.6 0.8 fusion.41
  10.5 0.7 maximum_maximum_fusion
  11.2 118.4 %all-gather.7.cloned.1.call-done = bf16[10240,256]{1,0:T(8,128)(2,1)} async-done(((bf16[80,256]{1,0:T(8,128)(2,1)}), bf16[10240,256]{1,0:T(8,128)(2,1)}) %all-gather.7.cloned.1.call-update) | async-done | bytes 5242896 | tf_op jit(solution)/shard_map/all_gather | solution.py:224
  129.5 4.2 %collective-permute-start = (bf16[32,4,80,256]{3,2,1,0:T(8,128)(2,1)}, bf16[32,4,80,256]{3,2,1,0:T(8,128)(2,1)}, u32[]{:S(2)}, u32[]{:S(2)}) collective-permute-start(bf16[32,4,80,256]{3,2,1,0:T(8,128)(2,1)} %bitcast.82), channel_id=1, source_target_pairs={{0,4},{4,0},{1,5},{5,1},{2,6},{6,2},{3,7},{7,3},{8,12},{12,8},{9,1... | collective-permute-start | bytes 15728648 | tf_op jit(solution)/shard_map/ppermute | solution.py:226
  133.8 0.9 copy.63
  135.0 1.0 copy.62
  136.3 0.7 pad_add_fusion.meta
  137.6 1.7 constant_dynamic-slice_fusion
  139.9 0.8 maximum_bitcast_fusion.q_ref
  140.7 5.2 %shard_map.172 = (f32[2,256,128]{2,1,0:T(8,128)}, f32[2,256,128]{2,1,0:T(8,128)}, f32[2,256,128]{2,1,0:T(8,128)}) custom-call(s32[4]{0:T(128)} %pad_add_fusion.1.meta, bf16[2,256,256]{2,1,0:T(8,128)(2,1)} %maximum_bitcast_fusion.q_ref, bf16[32,4,80,256]{3,2,1,0:T(8,128)(2,1)} %bitcast.83, bf16[256,256]{1,0:T(8,128)(2,1)} %get-tuple-element.28.ku_ref, ...), custom_call_target="tpu_custom_call" | custom-call | flops 3000000000 | bytes 6000000 | tf_op jit(solution)/shard_map/pallas_call | solution.py:175
  145.9 5.3 %shard_map.173 = bf16[256,256]{1,0:T(8,128)(2,1)} custom-call(s32[4]{0:T(128)} %pad_add_fusion.meta, bf16[2,256,256]{2,1,0:T(8,128)(2,1)} %maximum_bitcast_fusion.q_ref, bf16[32,4,80,256]{3,2,1,0:T(8,128)(2,1)} %collective-permute-done.g_ref, bf16[256,256]{1,0:T(8,128)(2,1)} %get-tuple-element.28.ku_ref, bf16[256,256]{1,0:T(8,128)(2,1)} %get-tuple-element.27.vu_ref, ...), custom_call_target="tpu_custom_call" | custom-call | flops 3000000000 | bytes 6000000 | tf_op jit(solution)/shard_map/pallas_call | solution.py:175
  151.2 2.3 convolution_convert_fusion.2
  153.5 4.1 %all-to-all-start = ((bf16[4,64,2048]{2,1,0:T(8,128)(2,1)}), bf16[4,64,2048]{2,1,0:T(8,128)(2,1)S(1)}, u32[]{:S(2)}, u32[]{:S(2)}) async-start(bf16[4,64,2048]{2,1,0:T(8,128)(2,1)} %bitcast.75), calls=%async_computation | async-start | bytes 2097152 | tf_op jit(solution)/shard_map/all_to_all | solution.py:262
  157.7 14.2 %all-to-all-done = bf16[4,64,2048]{2,1,0:T(8,128)(2,1)S(1)} async-done(((bf16[4,64,2048]{2,1,0:T(8,128)(2,1)}), bf16[4,64,2048]{2,1,0:T(8,128)(2,1)S(1)}, u32[]{:S(2)}, u32[]{:S(2)}) %all-to-all-start) | async-done | bytes 1048608 | tf_op jit(solution)/shard_map/all_to_all | solution.py:262
  172.3 0.8 fusion.32
  173.8 41.8 %all-gather.3 = f32[8,64,8]{1,2,0:T(8,128)S(1)} all-gather(f32[1,64,8]{1,2,0:T(8,128)S(1)} %maximum_bitcast_fusion.1), channel_id=3, replica_groups=mesh['z'=8,'x'=4,'core'=2,'y'=4] {'z'}, dimensions={0}, use_global_device_ids=true | all-gather | bytes 18432 | tf_op jit(solution)/shard_map/all_gather | solution.py:248
  215.9 13.4 %all-gather.9.cloned.1.call-done = bf16[512,2048]{1,0:T(8,128)(2,1)} async-done(((bf16[64,2048]{1,0:T(8,128)(2,1)}), bf16[512,2048]{1,0:T(8,128)(2,1)}) %all-gather.9.cloned.1.call-update) | async-done | bytes 2097168 | tf_op jit(solution)/shard_map/all_gather | solution.py:267
  229.3 2.3 fusion
  231.9 35.3 %all_to_all.15 = bf16[8,8,8,2048]{3,2,1,0:T(8,128)(2,1)S(1)} all-to-all(bf16[8,8,8,2048]{3,2,1,0:T(8,128)(2,1)S(1)} %bitcast.74), channel_id=1, replica_groups=mesh['z'=8,'x'=4,'core'=2,'y'=4] {'x','core'}, dimensions={0} | all-to-all | bytes 4194304 | tf_op jit(solution)/shard_map/all_to_all | solution.py:272
  267.2 1.3 copy-done.1
  268.6 1.2 fusion.12
  269.8 5.7 %convolution_convert_fusion = bf16[512,2048]{1,0:T(8,128)(2,1)} fusion(bf16[1,384,2048]{2,1,0:T(8,128)(2,1)S(1)} %copy-done, bf16[512,2048]{1,0:T(8,128)(2,1)} %bitcast.79, bf16[1,2048,384]{2,1,0:T(8,128)(2,1)} %param.31, f32[512,384]{1,0:T(8,128)S(1)} %fusion.12), kind=kOutput, calls=%fused_computation.1 | convolution fusion | flops 1612840960 | bytes 8126464 | tf_op jit(solution)/shard_map/dot_general | solution.py:277
  275.5 5.3 %all-to-all-start.2 = ((bf16[8,8,8,2048]{3,2,1,0:T(8,128)(2,1)}), bf16[8,8,8,2048]{3,2,1,0:T(8,128)(2,1)}, u32[]{:S(2)}, u32[]{:S(2)}) async-start(bf16[8,8,8,2048]{3,2,1,0:T(8,128)(2,1)} %bitcast.77), calls=%async_computation.2 | async-start | bytes 4194304 | tf_op jit(solution)/shard_map/all_to_all | solution.py:280
  281.4 25.7 %all-to-all-done.2 = bf16[8,8,8,2048]{3,2,1,0:T(8,128)(2,1)} async-done(((bf16[8,8,8,2048]{3,2,1,0:T(8,128)(2,1)}), bf16[8,8,8,2048]{3,2,1,0:T(8,128)(2,1)}, u32[]{:S(2)}, u32[]{:S(2)}) %all-to-all-start.2) | async-done | bytes 2097184 | tf_op jit(solution)/shard_map/all_to_all | solution.py:280
  307.1 2.3 fusion.5
  309.4 3.7 %add_convert_fusion = bf16[8,64,2048]{2,1,0:T(8,128)(2,1)} fusion(f32[8,64,2048]{2,1,0:T(8,128)S(1)} %fusion.5, f32[8,64,64]{2,1,0:T(8,128)S(1)} %select_reduce_fusion, bf16[8,8,8,2048]{3,2,1,0:T(8,128)(2,1)} %all-to-all-done.2), kind=kOutput, calls=%fused_computation | convolution fusion | flops 136445952 | bytes 8519680 | tf_op jit(solution)/shard_map/stk,skd->std/dot_general | solution.py:285
  313.1 1.9 fusion.65
  315.1 33.5 %reduce-scatter.2.cloned.1.call-done = bf16[1,64,2048]{2,1,0:T(8,128)(2,1)} async-done(((bf16[8,64,2048]{2,1,0:T(8,128)(2,1)}), bf16[1,64,2048]{2,1,0:T(8,128)(2,1)}) %reduce-scatter.2.cloned.1.call-update) | async-done | bytes 262160 | tf_op jit(solution)/shard_map/reduce_scatter | solution.py:288
  348.5 3.0 fusion.3
  (58 shorter events, 4.6 us)
Async XLA Ops:
  6.5 263.3 %copy-start = (bf16[1,384,2048]{2,1,0:T(8,128)(2,1)S(1)}, bf16[1,384,2048]{2,1,0:T(8,128)(2,1)}, u32[]{:S(2)}) copy-start(bf16[1,384,2048]{2,1,0:T(8,128)(2,1)} %param.32) | copy-start | bytes 4718596
  6.5 123.0 %all-gather.7.cloned.1.call-start = ((), (), s32[]{:S(2)}) async-start(), calls=%async_computation.5 | async-start | bytes 5283840 | tf_op jit(solution)/shard_map/all_gather | solution.py:224
  129.5 16.4 %collective-permute-start = (bf16[32,4,80,256]{3,2,1,0:T(8,128)(2,1)}, bf16[32,4,80,256]{3,2,1,0:T(8,128)(2,1)}, u32[]{:S(2)}, u32[]{:S(2)}) collective-permute-start(bf16[32,4,80,256]{3,2,1,0:T(8,128)(2,1)} %bitcast.82), channel_id=1, source_target_pairs={{0,4},{4,0},{1,5},{5,1},{2,6},{6,2},{3,7},{7,3},{8,12},{12,8},{9,1... | collective-permute-start | bytes 15728648 | tf_op jit(solution)/shard_map/ppermute | solution.py:226
  145.9 5.3 %copy-start.3 = (bf16[256,2048]{1,0:T(8,128)(2,1)S(1)}, bf16[256,2048]{1,0:T(8,128)(2,1)}, u32[]{:S(2)}) copy-start(bf16[256,2048]{1,0:T(8,128)(2,1)} %param.25) | copy-start | bytes 3145732
  151.2 6.5 %copy-start.6 = (bf16[2048]{0:T(1024)(128)(2,1)S(1)}, bf16[2048]{0:T(1024)(128)(2,1)}, u32[]{:S(2)}) copy-start(bf16[2048]{0:T(1024)(128)(2,1)} %param.27) | copy-start | bytes 12292
  153.5 18.5 %copy-start.4 = (bf16[64,2048]{1,0:T(8,128)(2,1)S(1)}, bf16[64,2048]{1,0:T(8,128)(2,1)}, u32[]{:S(2)}) copy-start(bf16[64,2048]{1,0:T(8,128)(2,1)} %param.26) | copy-start | bytes 786436
  153.5 18.4 %all-to-all-start = ((bf16[4,64,2048]{2,1,0:T(8,128)(2,1)}), bf16[4,64,2048]{2,1,0:T(8,128)(2,1)S(1)}, u32[]{:S(2)}, u32[]{:S(2)}) async-start(bf16[4,64,2048]{2,1,0:T(8,128)(2,1)} %bitcast.75), calls=%async_computation | async-start | bytes 2097152 | tf_op jit(solution)/shard_map/all_to_all | solution.py:262
  157.7 15.5 %copy-start.5 = (s32[64,4]{0,1:T(4,128)S(1)}, s32[64,4]{0,1:T(4,128)}, u32[]{:S(2)}) copy-start(s32[64,4]{0,1:T(4,128)} %param.28) | copy-start | bytes 3076
  157.7 16.1 %copy-start.7 = (f32[64,4]{0,1:T(4,128)S(1)}, f32[64,4]{0,1:T(4,128)}, u32[]{:S(2)}) copy-start(f32[64,4]{0,1:T(4,128)} %param.29) | copy-start | bytes 3076
  157.7 71.7 %all-gather.9.cloned.1.call-start = ((), (), s32[]{:S(2)}) async-start(), calls=%async_computation.6 | async-start | bytes 2359296 | tf_op jit(solution)/shard_map/all_gather | solution.py:267
  231.9 36.6 %copy-start.8 = (bf16[1,2048,384]{2,1,0:T(8,128)(2,1)S(1)}, bf16[1,2048,384]{2,1,0:T(8,128)(2,1)}, u32[]{:S(2)}) copy-start(bf16[1,2048,384]{2,1,0:T(8,128)(2,1)} %param.30) | copy-start | bytes 4718596
  267.2 1.3 copy-start.1
  275.5 31.6 %all-to-all-start.2 = ((bf16[8,8,8,2048]{3,2,1,0:T(8,128)(2,1)}), bf16[8,8,8,2048]{3,2,1,0:T(8,128)(2,1)}, u32[]{:S(2)}, u32[]{:S(2)}) async-start(bf16[8,8,8,2048]{3,2,1,0:T(8,128)(2,1)} %bitcast.77), calls=%async_computation.2 | async-start | bytes 4194304 | tf_op jit(solution)/shard_map/all_to_all | solution.py:280
  280.8 67.8 %reduce-scatter.2.cloned.1.call-start = ((), (), s32[]{:S(2)}) async-start(), calls=%async_computation.4 | async-start | bytes 2359296 | tf_op jit(solution)/shard_map/reduce_scatter | solution.py:288
  313.1 35.5 %copy-start.2 = (bf16[384,2048]{1,0:T(8,128)(2,1)S(1)}, bf16[384,2048]{1,0:T(8,128)(2,1)}, u32[]{:S(2)}) copy-start(bf16[384,2048]{1,0:T(8,128)(2,1)} %param.35) | copy-start | bytes 4718596
Sparse Core Ops, SparseCore 0:
  11.3 118.1 all-gather.6
  173.3 56.0 all-gather.8
  313.2 35.2 reduce-scatter.1

commit v2 on v1

--- a/solution.py
+++ b/solution.py
@@ -13,8 +13,6 @@
 NZ, NX, NC, NY = 8, 4, 2, 4
 CAP = 8
 ROWS = 256
-QUART = 64
-PACK = 80
 
 rope_base = 10000.0
 norm_eps = 1e-06
@@ -44,48 +42,140 @@
     ).astype(jnp.bfloat16)
 
 
-KB = 4
 LOG2E = 1.4426950408889634
-
-
-def attend_kernel(first, last, meta, q_ref, g_ref, ku_ref, vu_ref, *refs):
-    if first:
-        state_in = None
-        outs = refs[:1] if last else refs[:3]
-        m_ref, l_ref, acc_ref = refs[-3:]
-    else:
-        mi_ref, li_ref, ai_ref = refs[:3]
-        outs = refs[3:4] if last else refs[3:6]
-        m_ref, l_ref, acc_ref = refs[-3:]
-    i = pl.program_id(0)
-    nsteps = pl.num_programs(0)
-    q_sp = meta[0]
-    core = meta[1]
-    needed = meta[2]
-    whole = meta[3]
+MESH_ID = pl.DeviceIdType.MESH
+OFFS = (0, -1, 1, -2, 2, -3, 3, -4)
+HALF = 160
+
+
+def ring(value, size):
+    return lax.rem(value + size, size)
+
+
+def greet(partners):
+    barrier = pltpu.get_barrier_semaphore()
+    for dev in partners:
+        pl.semaphore_signal(barrier, inc=1, device_id=dev, device_id_type=MESH_ID)
+    pl.semaphore_wait(barrier, len(partners))
+
+
+def gather_attend_kernel(
+    pay_ref, tab_ref, q_ref, ku_ref, vu_ref, out_ref, tabs_ref,
+    G, T, m_ref, l_ref, acc_ref, recv, trecv, zsend, tsend, xsend, fsend, ysend, csend, lsem,
+):
+    z, x, c, y = (lax.axis_index(n) for n in ("z", "x", "core", "y"))
+    hm = lax.rem(y, 2)
+    ho = 1 - hm
+    up, down = {"z": ring(z + 1, NZ)}, {"z": ring(z - 1, NZ)}
+    right, left = {"x": ring(x + 1, NX)}, {"x": ring(x - 1, NX)}
+    above, below = {"y": ring(y + 1, NY)}, {"y": ring(y - 1, NY)}
+    mate = {"core": 1 - c}
+    xs = {0: x, -1: ring(x - 1, NX), 1: ring(x + 1, NX), 2: ring(x + 2, NX)}
+    ZZ = [ring(z + off, NZ) for off in OFFS]
+    greet([up, down, right, left, above, below, mate])
+
+    def piece(zz, xx, h, sem, dev):
+        slot = G.at[c, zz, xx, h]
+        return pltpu.make_async_remote_copy(
+            src_ref=slot, dst_ref=slot, send_sem=sem, recv_sem=recv.at[c, zz, xx, h],
+            device_id=dev, device_id_type=MESH_ID,
+        )
+
+    def arrived(par, zz, xx, h):
+        slot = G.at[par, zz, xx, h]
+        pltpu.make_async_remote_copy(
+            src_ref=slot, dst_ref=slot, send_sem=csend, recv_sem=recv.at[par, zz, xx, h],
+            device_id=mate, device_id_type=MESH_ID,
+        ).wait_recv()
+
+    sent = []
+
+    def send(zz, xx, h, sems, at, dev):
+        piece(zz, xx, h, sems.at[at], dev).start()
+        sent.append(lambda: piece(zz, xx, h, sems.at[at], dev).wait_send())
+
+    def to_mate(zz, xx, h):
+        piece(zz, xx, h, csend, mate).start()
+
+    def table(zz, sem, dev):
+        return pltpu.make_async_remote_copy(
+            src_ref=T.at[zz], dst_ref=T.at[zz], send_sem=sem, recv_sem=trecv.at[zz],
+            device_id=dev, device_id_type=MESH_ID,
+        )
+
+    def send_table(zz, at, dev):
+        table(zz, tsend.at[at], dev).start()
+        sent.append(lambda: table(zz, tsend.at[at], dev).wait_send())
+
+    def ev_z(i):
+        off = OFFS[i]
+        zz = ZZ[i]
+        for h in range(2):
+            if i > 0:
+                arrived(c, zz, x, h)
+            if -4 < off <= 0:
+                send(zz, x, h, zsend, (0, -off, h), up)
+            if 0 <= off < 3:
+                send(zz, x, h, zsend, (1, off, h), down)
+            to_mate(zz, x, h)
+        send(zz, x, hm, xsend, (i, 0), right)
+        send(zz, x, hm, xsend, (i, 1), left)
+        if i > 0:
+            table(zz, tsend.at[0, 0], up).wait_recv()
+        if -4 < off <= 0:
+            send_table(zz, (0, -off), up)
+        if 0 <= off < 3:
+            send_table(zz, (1, off), down)
+
+    def to_y(i, j, zz, xx):
+        send(zz, xx, hm, ysend, (i, j), above if (i + j) % 2 == 0 else below)
+
+    def ev_x1(i):
+        zz = ZZ[i]
+        arrived(c, zz, xs[-1], hm)
+        if i % 2 == 0:
+            send(zz, xs[-1], hm, fsend, (i,), right)
+        to_y(i, 0, zz, xs[-1])
+        to_mate(zz, xs[-1], hm)
+        arrived(c, zz, xs[1], hm)
+        if i % 2 == 1:
+            send(zz, xs[1], hm, fsend, (i,), left)
+        to_y(i, 1, zz, xs[1])
+        to_mate(zz, xs[1], hm)
+
+    def ev_x2(i):
+        zz = ZZ[i]
+        arrived(c, zz, xs[2], hm)
+        to_y(i, 2, zz, xs[2])
+        to_mate(zz, xs[2], hm)
+
+    def ev_y(i, dx):
+        zz = ZZ[i]
+        arrived(c, zz, xs[dx], ho)
+        to_mate(zz, xs[dx], ho)
+
+    own = pltpu.make_async_copy(pay_ref, G.at[c, z, x], lsem.at[0])
+    own_table = pltpu.make_async_copy(tab_ref, T.at[z], lsem.at[1])
+    own.start()
+    own_table.start()
+    own.wait()
+    own_table.wait()
+
+    m_ref[...] = jnp.full(m_ref.shape, -1e30, jnp.float32)
+    l_ref[...] = jnp.zeros(l_ref.shape, jnp.float32)
+    acc_ref[...] = jnp.zeros(acc_ref.shape, jnp.float32)
     scale = LOG2E / math.sqrt(NOPE + ROPE)
-
-    @pl.when(i == 0)
-    def _():
-        if first:
-            m_ref[...] = jnp.full(m_ref.shape, -1e30, jnp.float32)
-            l_ref[...] = jnp.zeros(l_ref.shape, jnp.float32)
-            acc_ref[...] = jnp.zeros(acc_ref.shape, jnp.float32)
-        else:
-            m_ref[...] = mi_ref[...]
-            l_ref[...] = li_ref[...]
-            acc_ref[...] = ai_ref[...]
-
-    def step(masked):
-        keys = KB * ROWS
+    keys = 512
+
+    def compute(zz, xx, masked):
         lat = jnp.concatenate(
-            [g_ref[b, y, 0:QUART, :] for b in range(KB) for y in range(NY)], axis=0
+            [G[par, zz, xx, h, 0:128, :] for par in range(2) for h in range(2)], axis=0
         )
         rope = jnp.concatenate(
             [
-                g_ref[b, y, QUART:PACK, g * ROPE : (g + 1) * ROPE]
-                for b in range(KB)
-                for y in range(NY)
+                G[par, zz, xx, h, 128:HALF, g * ROPE : (g + 1) * ROPE]
+                for par in range(2)
+                for h in range(2)
                 for g in range(4)
             ],
             axis=0,
@@ -94,10 +184,8 @@
         k = jnp.dot(lat, ku_ref[...], preferred_element_type=jnp.float32).astype(jnp.bfloat16)
         v = jnp.dot(lat, vu_ref[...], preferred_element_type=jnp.float32).astype(jnp.bfloat16)
         if masked:
-            j = lax.broadcasted_iota(jnp.int32, (1, keys), 1)
-            chunk = i * KB + j // ROWS
-            kpos = (chunk * 2 + core) * ROWS + j % ROWS
-            qpos = q_sp * ROWS + lax.broadcasted_iota(jnp.int32, (ROWS, 1), 0)
+            kpos = lax.broadcasted_iota(jnp.int32, (1, keys), 1)
+            qpos = c * ROWS + lax.broadcasted_iota(jnp.int32, (ROWS, 1), 0)
             allowed = kpos <= qpos
         for h in range(2):
             kcat = jnp.concatenate([k[:, h * NOPE : (h + 1) * NOPE], rope], axis=1)
@@ -121,72 +209,93 @@
             )
             m_ref[h] = m_new
 
-    @pl.when(i < whole)
-    def _():
-        step(False)
-
-    @pl.when((i >= whole) & (i < needed))
-    def _():
-        step(True)
-
-    @pl.when(i == nsteps - 1)
-    def _():
-        if last:
-            for h in range(2):
-                outs[0][:, h * VDIM : (h + 1) * VDIM] = (acc_ref[h] / l_ref[h]).astype(jnp.bfloat16)
-        else:
-            outs[0][...] = m_ref[...]
-            outs[1][...] = l_ref[...]
-            outs[2][...] = acc_ref[...]
-
-
-def attend(q_cat, gathered, key_local, value_local, q_sp, core, state):
-    first = state is None
-    last = not first
-    have = jnp.maximum((q_sp - core) // 2 + 1, 0)
-    have = jnp.where(q_sp < core, 0, have)
-    needed = (have + KB - 1) // KB
-    full = jnp.where(q_sp <= core, 0, (q_sp - core + 1) // 2)
-    whole = full // KB
-    meta = jnp.stack([q_sp, core, needed, whole]).astype(jnp.int32)
-    nsteps = (NZ * NX) // KB
-    state_spec = pl.BlockSpec((2, ROWS, 128), lambda i, meta: (0, 0, 0))
-    in_specs = [
-        pl.BlockSpec((2, ROWS, 256), lambda i, meta: (0, 0, 0)),
-        pl.BlockSpec(
-            (KB, NY, PACK, 256),
-            lambda i, meta: (jnp.minimum(i, jnp.maximum(meta[2] - 1, 0)), 0, 0, 0),
+    mine = z * NX + x
+
+    def round_(s, carry):
+        for k in range(11):
+
+            @pl.when(s == k)
+            def _():
+                if k < 8:
+                    ev_z(k)
+                if 0 <= k - 1 < 8:
+                    ev_x1(k - 1)
+                if 0 <= k - 2 < 8:
+                    ev_x2(k - 2)
+                    ev_y(k - 2, -1)
+                    ev_y(k - 2, 1)
+                if 0 <= k - 3 < 8:
+                    ev_y(k - 3, 2)
+
+        def pair(d, carry):
+            i = s - 1 - jnp.where(d == 0, 0, jnp.where(d == 3, 3, 2))
+
+            @pl.when((i >= 0) & (i < 8))
+            def _():
+                off = jnp.where(lax.rem(i, 2) == 1, -((i + 1) // 2), i // 2)
+                dx = jnp.where(d == 3, 2, jnp.where(d == 1, -1, jnp.where(d == 2, 1, 0)))
+                zz = ring(z + off, NZ)
+                xx = ring(x + dx, NX)
+                for h in range(2):
+                    arrived(1 - c, zz, xx, h)
+                theirs = zz * NX + xx
+
+                @pl.when(theirs < mine)
+                def _():
+                    compute(zz, xx, False)
+
+                @pl.when(theirs == mine)
+                def _():
+                    compute(zz, xx, True)
+
+            return carry
+
+        return lax.fori_loop(0, 4, pair, carry)
+
+    lax.fori_loop(0, 12, round_, 0)
+
+    for h in range(2):
+        out_ref[:, h * VDIM : (h + 1) * VDIM] = (acc_ref[h] / l_ref[h]).astype(jnp.bfloat16)
+    tabs_ref[...] = T[...]
+    for wait in sent:
+        wait()
+    whole = G.at[c]
+    pltpu.make_async_remote_copy(
+        src_ref=whole, dst_ref=whole, send_sem=csend, recv_sem=recv.at[0, 0, 0, 0],
+        device_id=mate, device_id_type=MESH_ID,
+    ).wait_send()
+
+
+def gather_attend(payload, tables, q_cat, key_local, value_local):
+    vmem = pl.BlockSpec(memory_space=pltpu.VMEM)
+    return pl.pallas_call(
+        gather_attend_kernel,
+        out_shape=(
+            jax.ShapeDtypeStruct((ROWS, 256), jnp.bfloat16),
+            jax.ShapeDtypeStruct((NZ, 8, 128), jnp.float32),
         ),
-        pl.BlockSpec((256, 256), lambda i, meta: (0, 0)),
-        pl.BlockSpec((256, 256), lambda i, meta: (0, 0)),
-    ]
-    args = [q_cat, gathered, key_local, value_local]
-    if not first:
-        in_specs += [state_spec] * 3
-        args += list(state)
-    if last:
-        out_shape = jax.ShapeDtypeStruct((ROWS, 256), jnp.bfloat16)
-        out_specs = pl.BlockSpec((ROWS, 256), lambda i, meta: (0, 0))
-    else:
-        out_shape = tuple(jax.ShapeDtypeStruct((2, ROWS, 128), jnp.float32) for _ in range(3))
-        out_specs = (state_spec,) * 3
-    import functools
-
-    return pl.pallas_call(
-        functools.partial(attend_kernel, first, last),
-        out_shape=out_shape,
-        grid_spec=pltpu.PrefetchScalarGridSpec(
-            num_scalar_prefetch=1,
-            grid=(nsteps,),
-            in_specs=in_specs,
-            out_specs=out_specs,
-            scratch_shapes=[pltpu.VMEM((2, ROWS, 128), jnp.float32)] * 3,
+        in_specs=[vmem] * 5,
+        out_specs=(vmem, vmem),
+        scratch_shapes=[
+            pltpu.VMEM((2, NZ, NX, 2, HALF, 256), jnp.bfloat16),
+            pltpu.VMEM((NZ, 8, 128), jnp.float32),
+            pltpu.VMEM((2, ROWS, 128), jnp.float32),
+            pltpu.VMEM((2, ROWS, 128), jnp.float32),
+            pltpu.VMEM((2, ROWS, 128), jnp.float32),
+            pltpu.SemaphoreType.DMA((2, NZ, NX, 2)),
+            pltpu.SemaphoreType.DMA((NZ,)),
+            pltpu.SemaphoreType.DMA((2, 4, 2)),
+            pltpu.SemaphoreType.DMA((2, 4)),
+            pltpu.SemaphoreType.DMA((8, 2)),
+            pltpu.SemaphoreType.DMA((8,)),
+            pltpu.SemaphoreType.DMA((8, 3)),
+            pltpu.SemaphoreType.DMA,
+            pltpu.SemaphoreType.DMA((2,)),
+        ],
+        compiler_params=pltpu.CompilerParams(
+            collective_id=0, has_side_effects=True, vmem_limit_bytes=40 * 1024 * 1024
         ),
-        compiler_params=pltpu.CompilerParams(dimension_semantics=("arbitrary",)),
-        cost_estimate=pl.CostEstimate(
-            flops=3_000_000_000, bytes_accessed=6_000_000, transcendentals=4_000_000
-        ),
-    )(meta, *args)
+    )(payload, tables, q_cat, key_local, value_local)
 
 
 def body(
@@ -214,16 +323,10 @@
     first_row = q_sp * ROWS
     positions = first_row + jnp.arange(ROWS, dtype=jnp.int32)
 
-    lat_q = lax.dynamic_slice_in_dim(latent, y * QUART, QUART, 0)
-    rope_q = lax.dynamic_slice_in_dim(key_rope, y * QUART, QUART, 0)
-    pos_q = first_row + y * QUART + jnp.arange(QUART, dtype=jnp.int32)
-    normed_latent = scale_rows(lat_q, latent_gain)
-    rot_key = rotate(rope_q[:, None, :], pos_q)[:, 0, :]
-    packed_rope = jnp.concatenate([rot_key[g * 16 : (g + 1) * 16] for g in range(4)], axis=1)
-    payload = jnp.concatenate([normed_latent, packed_rope], axis=0)
-    mine = lax.all_gather(payload, ("z", "x", "y"), axis=0, tiled=False)
-    mine = mine.reshape(NZ * NX, NY, PACK, 256)
-    theirs = lax.ppermute(mine, "core", [(0, 1), (1, 0)])
+    normed_latent = scale_rows(latent, latent_gain)
+    rot_key = rotate(key_rope[:, None, :], positions)[:, 0, :]
+    packed = rot_key.reshape(2, 4, 32, ROPE).transpose(0, 2, 1, 3).reshape(2, 32, 256)
+    payload = jnp.concatenate([normed_latent.reshape(2, 128, 256), packed], axis=1)
 
     key_local = lax.dynamic_slice_in_dim(key_up, y * 256, 256, 1)
     value_local = lax.dynamic_slice_in_dim(value_up, y * 256, 256, 1)
@@ -245,7 +348,9 @@
     before = jnp.dot(earlier, onehot)
     rank = jnp.sum(before * onehot, axis=1).reshape(64, 4)
     tables = jnp.concatenate([expert_ids.astype(jnp.float32) * CAP + rank, route_weights], axis=1)
-    tables = lax.all_gather(tables, "z", axis=0, tiled=False)
+    tables = jnp.concatenate([tables.T, jnp.zeros((8, 64), jnp.float32)], axis=1)
+    heads_out, gathered = gather_attend(payload, tables, q_cat, key_local, value_local)
+    tables = gathered[:, :, :64].transpose(0, 2, 1)
     slot_of = tables[:, :, :4] - (z * 64).astype(jnp.float32)
     weight_of = tables[:, :, 4:]
     slots = jnp.arange(64, dtype=jnp.float32)
@@ -254,9 +359,6 @@
     share = jnp.sum(jnp.where(hit, weight_of[:, :, :, None], 0.0), axis=2)
     share_hi = share.astype(jnp.bfloat16)
     share_lo = (share - share_hi.astype(jnp.float32)).astype(jnp.bfloat16)
-
-    state = attend(q_cat, mine, key_local, value_local, q_sp, core, None)
-    heads_out = attend(q_cat, theirs, key_local, value_local, q_sp, 1 - core, state)
 
     part = jnp.dot(heads_out, out_proj, preferred_element_type=jnp.float32).astype(jnp.bfloat16)
     pieces = lax.all_to_all(part.reshape(4, 64, 2048), "y", 0, 0, tiled=True)

time: 363 us -> 268 us (0.74)
  waiting for transfers between devices: 205 us -> 119 us
  blocking collectives: 77.1 us -> 35.2 us
  Pallas kernels: 10.4 us -> 51.3 us
  starting transfers between devices: 13.7 us -> 9.5 us
    all_gather x1 -> x0, waiting for transfers between devices: 118 us -> none  [body(): mine = lax.all_gather(payload, ('z', 'x', 'y'), axis=0, tiled=False)]
    all_gather x1 -> x0, blocking collectives: 41.8 us -> none  [body(): tables = lax.all_gather(tables, 'z', axis=0, tiled=False)]
    pallas_call x2 -> x1, Pallas kernels: 10.4 us -> 51.3 us  [gather_attend(): pl.pallas_call(gather_attend_kernel, out_shape=(jax.ShapeDtypeStruct((ROW...]
    all_gather x1, waiting for transfers between devices: 13.4 us -> 44.7 us  [body(): column = lax.all_gather(normed, 'z', axis=0, tiled=False)]
    ppermute x1 -> x0, starting transfers between devices: 4.25 us -> none  [body(): theirs = lax.ppermute(mine, 'core', [(0, 1), (1, 0)])]
  transfers between devices with their start and end apart: 6 -> 4, of which waited for: 5 -> 4; matrix products, arithmetic and copies ran while one was open for 3% -> 1% of each run, Pallas kernels for 1% -> 0%
where the time goes in v2:
time: 268 us; the launch traced here: 264 us
  waiting for transfers between devices  119 us (44%)
  Pallas kernels  51.3 us (19%)
  blocking collectives  35.2 us (13%)
  matrix products  21.8 us (8%)
  between operations  13.7 us (5%)
  starting transfers between devices  9.5 us (4%)
  other arithmetic  6.79 us (3%)
  local copies, waits for them, and re-layouts  6.75 us (3%)
    pallas_call x1, Pallas kernels, gather_attend(): pl.pallas_call(gather_attend_kernel, out_shape=(jax.ShapeDtypeStruct((ROW...  51.3 us
    all_gather x1, waiting for transfers between devices, body(): column = lax.all_gather(normed, 'z', axis=0, tiled=False)  44.7 us
    all_to_all x1, blocking collectives, body(): lax.all_to_all(outgoing, ('x', 'core'), split_axis=0, concat_axis=0, tile...  35.2 us
    reduce_scatter x1, waiting for transfers between devices, body(): lax.psum_scatter(partial.astype(jnp.bfloat16), 'z', scatter_dimension=0,...  33.3 us
    all_to_all x1, waiting for transfers between devices, body(): lax.all_to_all(expert_rows.reshape(8, 8, CAP, 2048), ('x', 'core'), split...  25.7 us
    all_to_all x1, waiting for transfers between devices, body(): pieces = lax.all_to_all(part.reshape(4, 64, 2048), 'y', 0, 0, tiled=True)  14.9 us
    dot_general x1, matrix products, body(): jnp.dot(expert_hidden, expert_down[0], preferred_element_type=jnp.float32)  5.69 us
  transfers between devices with their start and end apart: 4, of which 4 were waited for; matrix products, arithmetic and copies ran while one was open for 1% of the time, Pallas kernels for 0%

profile of v2, /device:TPU:1, one launch (start us, length us, event | category | flops | bytes accessed | tf_op | source)
XLA Modules:
  0.0 263.7 jit_solution(15854002626591897750)
XLA Ops:
  6.6 1.1 copy.42
  7.9 1.0 copy.41
  9.0 0.8 copy.45
  9.7 0.8 bitcast_convert_fusion
  10.5 1.2 multiply_cosine_fusion
  11.7 0.2 fusion.50
  13.0 0.2 fusion.21
  13.7 1.0 constant_dynamic-slice_fusion
  14.7 1.0 subtract_convert_fusion.1
  15.7 1.0 maximum_bitcast_fusion.q_ref
  16.7 51.3 %shard_map.172 = (bf16[256,256]{1,0:T(8,128)(2,1)S(1)}, f32[8,8,128]{2,1,0:T(8,128)S(1)}) custom-call(bf16[2,160,256]{2,1,0:T(8,128)(2,1)S(1)} %pad_maximum_fusion.pay_ref, f32[8,128]{1,0:T(8,128)S(1)} %concatenate.31.tab_ref, bf16[2,256,256]{2,1,0:T(8,128)(2,1)S(1)} %maximum_bitcast_fusion.q_ref, bf16[256,256]{1,0:T(8,128)(2,1)S(1)} %get-tuple-element.22.ku_ref, ...), custom_call_target="tpu_custom_call" | custom-call | tf_op jit(solution)/shard_map/pallas_call | solution.py:271
  68.0 1.4 convolution_convert_fusion.2
  69.4 4.2 %all-to-all-start = ((bf16[4,64,2048]{2,1,0:T(8,128)(2,1)}), bf16[4,64,2048]{2,1,0:T(8,128)(2,1)S(1)}, u32[]{:S(2)}, u32[]{:S(2)}) async-start(bf16[4,64,2048]{2,1,0:T(8,128)(2,1)} %bitcast.68), calls=%async_computation | async-start | bytes 2097152 | tf_op jit(solution)/shard_map/all_to_all | solution.py:364
  73.7 14.9 %all-to-all-done = bf16[4,64,2048]{2,1,0:T(8,128)(2,1)S(1)} async-done(((bf16[4,64,2048]{2,1,0:T(8,128)(2,1)}), bf16[4,64,2048]{2,1,0:T(8,128)(2,1)S(1)}, u32[]{:S(2)}, u32[]{:S(2)}) %all-to-all-start) | async-done | bytes 1048608 | tf_op jit(solution)/shard_map/all_to_all | solution.py:364
  88.8 0.2 fusion.30
  88.9 0.8 fusion.32
  89.8 0.3 fusion.22
  90.2 44.7 %all-gather.3.cloned.1.call-done = bf16[512,2048]{1,0:T(8,128)(2,1)} async-done(((bf16[64,2048]{1,0:T(8,128)(2,1)}), bf16[512,2048]{1,0:T(8,128)(2,1)}) %all-gather.3.cloned.1.call-update) | async-done | bytes 2097168 | tf_op jit(solution)/shard_map/all_gather | solution.py:369
  134.9 2.3 fusion
  137.3 0.2 copy.61
  137.5 35.2 %all_to_all.15 = bf16[8,8,8,2048]{3,2,1,0:T(8,128)(2,1)S(1)} all-to-all(bf16[8,8,8,2048]{3,2,1,0:T(8,128)(2,1)S(1)} %bitcast.67), channel_id=1, replica_groups=mesh['z'=8,'x'=4,'core'=2,'y'=4] {'x','core'}, dimensions={0} | all-to-all | bytes 4194304 | tf_op jit(solution)/shard_map/all_to_all | solution.py:374
  172.7 1.3 copy-done.1
  174.1 1.2 fusion.12
  175.3 5.7 %convolution_convert_fusion = bf16[512,2048]{1,0:T(8,128)(2,1)} fusion(bf16[1,384,2048]{2,1,0:T(8,128)(2,1)S(1)} %copy-done, bf16[512,2048]{1,0:T(8,128)(2,1)} %bitcast.72, bf16[1,2048,384]{2,1,0:T(8,128)(2,1)} %param.31, f32[512,384]{1,0:T(8,128)S(1)} %fusion.12), kind=kOutput, calls=%fused_computation.1 | convolution fusion | flops 1612840960 | bytes 8126464 | tf_op jit(solution)/shard_map/dot_general | solution.py:379
  181.0 5.3 %all-to-all-start.2 = ((bf16[8,8,8,2048]{3,2,1,0:T(8,128)(2,1)}), bf16[8,8,8,2048]{3,2,1,0:T(8,128)(2,1)}, u32[]{:S(2)}, u32[]{:S(2)}) async-start(bf16[8,8,8,2048]{3,2,1,0:T(8,128)(2,1)} %bitcast.70), calls=%async_computation.2 | async-start | bytes 4194304 | tf_op jit(solution)/shard_map/all_to_all | solution.py:382
  186.3 0.6 select_reduce_fusion
  186.9 25.7 %all-to-all-done.2 = bf16[8,8,8,2048]{3,2,1,0:T(8,128)(2,1)} async-done(((bf16[8,8,8,2048]{3,2,1,0:T(8,128)(2,1)}), bf16[8,8,8,2048]{3,2,1,0:T(8,128)(2,1)}, u32[]{:S(2)}, u32[]{:S(2)}) %all-to-all-start.2) | async-done | bytes 2097184 | tf_op jit(solution)/shard_map/all_to_all | solution.py:382
  212.6 2.3 fusion.5
  214.9 3.7 %add_convert_fusion = bf16[8,64,2048]{2,1,0:T(8,128)(2,1)} fusion(f32[8,64,2048]{2,1,0:T(8,128)S(1)} %fusion.5, f32[8,64,64]{2,1,0:T(8,128)S(1)} %select_reduce_fusion, bf16[8,8,8,2048]{3,2,1,0:T(8,128)(2,1)} %all-to-all-done.2), kind=kOutput, calls=%fused_computation | convolution fusion | flops 136445952 | bytes 8519680 | tf_op jit(solution)/shard_map/stk,skd->std/dot_general | solution.py:387
  218.6 1.9 fusion.58
  220.5 33.3 %reduce-scatter.2.cloned.1.call-done = bf16[1,64,2048]{2,1,0:T(8,128)(2,1)} async-done(((bf16[8,64,2048]{2,1,0:T(8,128)(2,1)}), bf16[1,64,2048]{2,1,0:T(8,128)(2,1)}) %reduce-scatter.2.cloned.1.call-update) | async-done | bytes 262160 | tf_op jit(solution)/shard_map/reduce_scatter | solution.py:390
  253.9 3.0 %fusion.3 = bf16[64,2048]{1,0:T(8,128)(2,1)} fusion(bf16[384,2048]{1,0:T(8,128)(2,1)S(1)} %copy-done.2, bf16[2048,384]{1,0:T(8,128)(2,1)} %param.34, bf16[64,2048]{1,0:T(8,128)(2,1)S(1)} %get-tuple-element.10, bf16[1,64,2048]{2,1,0:T(8,128)(2,1)} %reduce-scatter.2.cloned.1.call-done, f32[64,384]{1,0:T(8,128)S(1)} %fusion.58, ...), kind=kOutput, calls=%fused_computation.8 | convolution fusion | flops 202915840 | bytes 4038912 | tf_op jit(solution)/shard_map/dot_general | solution.py:397
  (55 shorter events, 2.0 us)
Async XLA Ops:
  6.5 168.8 %copy-start = (bf16[1,384,2048]{2,1,0:T(8,128)(2,1)S(1)}, bf16[1,384,2048]{2,1,0:T(8,128)(2,1)}, u32[]{:S(2)}) copy-start(bf16[1,384,2048]{2,1,0:T(8,128)(2,1)} %param.32) | copy-start | bytes 4718596
  6.5 6.1 %copy-start.4 = (bf16[256,256]{1,0:T(8,128)(2,1)S(1)}, bf16[256,256]{1,0:T(8,128)(2,1)}, u32[]{:S(2)}) copy-start(bf16[256,256]{1,0:T(8,128)(2,1)} %param.20) | copy-start | bytes 393220
  6.5 6.2 %copy-start.10 = (bf16[256]{0:T(256)(128)(2,1)S(1)}, bf16[256]{0:T(256)(128)(2,1)}, u32[]{:S(2)}) copy-start(bf16[256]{0:T(256)(128)(2,1)} %param.22) | copy-start | bytes 1540
  6.5 6.3 %copy-start.6 = (s32[64,4]{0,1:T(4,128)S(1)}, s32[64,4]{0,1:T(4,128)}, u32[]{:S(2)}) copy-start(s32[64,4]{0,1:T(4,128)} %param.28) | copy-start | bytes 3076
  6.5 7.1 %copy-start.8 = (f32[64,4]{0,1:T(4,128)S(1)}, f32[64,4]{0,1:T(4,128)}, u32[]{:S(2)}) copy-start(f32[64,4]{0,1:T(4,128)} %param.29) | copy-start | bytes 3076
  12.4 55.6 %copy-start.3 = (bf16[256,2048]{1,0:T(8,128)(2,1)S(1)}, bf16[256,2048]{1,0:T(8,128)(2,1)}, u32[]{:S(2)}) copy-start(bf16[256,2048]{1,0:T(8,128)(2,1)} %param.25) | copy-start | bytes 3145732
  68.0 5.7 %copy-start.7 = (bf16[2048]{0:T(1024)(128)(2,1)S(1)}, bf16[2048]{0:T(1024)(128)(2,1)}, u32[]{:S(2)}) copy-start(bf16[2048]{0:T(1024)(128)(2,1)} %param.27) | copy-start | bytes 12292
  69.4 19.3 %copy-start.5 = (bf16[64,2048]{1,0:T(8,128)(2,1)S(1)}, bf16[64,2048]{1,0:T(8,128)(2,1)}, u32[]{:S(2)}) copy-start(bf16[64,2048]{1,0:T(8,128)(2,1)} %param.26) | copy-start | bytes 786436
  69.4 19.1 %all-to-all-start = ((bf16[4,64,2048]{2,1,0:T(8,128)(2,1)}), bf16[4,64,2048]{2,1,0:T(8,128)(2,1)S(1)}, u32[]{:S(2)}, u32[]{:S(2)}) async-start(bf16[4,64,2048]{2,1,0:T(8,128)(2,1)} %bitcast.68), calls=%async_computation | async-start | bytes 2097152 | tf_op jit(solution)/shard_map/all_to_all | solution.py:364
  73.7 61.2 %all-gather.3.cloned.1.call-start = ((), (), s32[]{:S(2)}) async-start(), calls=%async_computation.5 | async-start | bytes 2359296 | tf_op jit(solution)/shard_map/all_gather | solution.py:369
  137.5 36.6 %copy-start.9 = (bf16[1,2048,384]{2,1,0:T(8,128)(2,1)S(1)}, bf16[1,2048,384]{2,1,0:T(8,128)(2,1)}, u32[]{:S(2)}) copy-start(bf16[1,2048,384]{2,1,0:T(8,128)(2,1)} %param.30) | copy-start | bytes 4718596
  172.7 1.3 copy-start.1
  181.0 31.6 %all-to-all-start.2 = ((bf16[8,8,8,2048]{3,2,1,0:T(8,128)(2,1)}), bf16[8,8,8,2048]{3,2,1,0:T(8,128)(2,1)}, u32[]{:S(2)}, u32[]{:S(2)}) async-start(bf16[8,8,8,2048]{3,2,1,0:T(8,128)(2,1)} %bitcast.70), calls=%async_computation.2 | async-start | bytes 4194304 | tf_op jit(solution)/shard_map/all_to_all | solution.py:382
  186.3 67.6 %reduce-scatter.2.cloned.1.call-start = ((), (), s32[]{:S(2)}) async-start(), calls=%async_computation.4 | async-start | bytes 2359296 | tf_op jit(solution)/shard_map/reduce_scatter | solution.py:390
  218.6 35.3 %copy-start.2 = (bf16[384,2048]{1,0:T(8,128)(2,1)S(1)}, bf16[384,2048]{1,0:T(8,128)(2,1)}, u32[]{:S(2)}) copy-start(bf16[384,2048]{1,0:T(8,128)(2,1)} %param.35) | copy-start | bytes 4718596
Sparse Core Ops, SparseCore 0:
  89.9 44.9 all-gather.2
  218.7 35.1 reduce-scatter.1

commit v3 on v2

--- a/solution.py
+++ b/solution.py
@@ -298,6 +298,221 @@
     )(payload, tables, q_cat, key_local, value_local)
 
 
+def moe_kernel(
+    norm_ref, hid_ref, tab_ref, wg_h, wu_h, wd_h, sg_h, su_h, sd_h, out_ref,
+    COL, OUT, ARR, EO, RET, PART, RD, RU, wg, wu, wd, sg, su, sd,
+    zrecv, zsend, arecv, asend, rrecv, rsend, drecv, dsend, lsem, wsem,
+):
+    z, x, c, y = (lax.axis_index(n) for n in ("z", "x", "core", "y"))
+    me = x * NC + c
+    up, down = {"z": ring(z + 1, NZ)}, {"z": ring(z - 1, NZ)}
+    peers = []
+    for q in range(1, 8):
+        p = ring(me + q, 8)
+        peers.append((p, {"x": p // NC, "core": lax.rem(p, NC)}))
+
+    weights = [
+        pltpu.make_async_copy(src, dst, wsem.at[n])
+        for n, (src, dst) in enumerate(
+            ((sg_h, sg), (su_h, su), (sd_h, sd), (wg_h, wg), (wu_h, wu), (wd_h, wd))
+        )
+    ]
+    own = pltpu.make_async_copy(norm_ref, COL.at[0], lsem.at[0])
+    own.start()
+    for w in weights:
+        w.start()
+    greet([up, down] + [dev for _, dev in peers])
+    own.wait()
+
+    at = {off: i for i, off in enumerate(OFFS)}
+
+    def along_z(i, dev, off_to, sems, n):
+        return pltpu.make_async_remote_copy(
+            src_ref=COL.at[i], dst_ref=COL.at[at[off_to]], send_sem=sems.at[n],
+            recv_sem=zrecv.at[at[off_to]], device_id=dev, device_id_type=MESH_ID,
+        )
+
+    sends = []
+
+    def start(copy):
+        copy.start()
+        sends.append(copy)
+
+    def pieces(i, src, dst, sems_send, sems_recv):
+        for p, dev in peers:
+            pltpu.make_async_remote_copy(
+                src_ref=src.at[i, p], dst_ref=dst.at[i, me], send_sem=sems_send.at[i],
+                recv_sem=sems_recv.at[i], device_id=dev, device_id_type=MESH_ID,
+            ).start()
+        pltpu.make_async_copy(src.at[i, me], dst.at[i, me], lsem.at[1]).start()
+        pltpu.make_async_copy(src.at[i, me], dst.at[i, me], lsem.at[1]).wait()
+
+    def pieces_in(i, dst, sems_recv):
+        ref = dst.at[i, 0:7]
+        pltpu.make_async_remote_copy(
+            src_ref=ref, dst_ref=ref, send_sem=lsem.at[2], recv_sem=sems_recv.at[i],
+            device_id=peers[0][1], device_id_type=MESH_ID,
+        ).wait_recv()
+
+    def pieces_sent(i, src, sems_send):
+        ref = src.at[i, 0:7]
+        pltpu.make_async_remote_copy(
+            src_ref=ref, dst_ref=ref, send_sem=sems_send.at[i], recv_sem=lsem.at[2],
+            device_id=peers[0][1], device_id_type=MESH_ID,
+        ).wait_send()
+
+    slots = lax.broadcasted_iota(jnp.int32, (64, 64), 0).astype(jnp.float32)
+
+    def matches(i):
+        tab = tab_ref[ring(z + OFFS[i], NZ)]
+        base = (z * 64).astype(jnp.float32)
+        return [(tab[k : k + 1, 0:64] - base) == slots for k in range(4)], tab
+
+    def arrive(i):
+        off = OFFS[i]
+        if i > 0:
+            along_z(i, up, off, zsend, 0).wait_recv()
+        if -4 < off <= 0:
+            start(along_z(i, up, off - 1, zsend, -off))
+        if 0 <= off < 3:
+            start(along_z(i, down, off + 1, zsend, 4 + off))
+        hit, _ = matches(i)
+        pick = jnp.where(hit[0] | hit[1] | hit[2] | hit[3], 1.0, 0.0).astype(jnp.bfloat16)
+        rows = jnp.dot(pick, COL[i], preferred_element_type=jnp.float32)
+        for p in range(8):
+            OUT[i, p] = rows[p * CAP : (p + 1) * CAP].astype(jnp.bfloat16)
+        pieces(i, OUT, ARR, asend, arecv)
+
+    def gated(rows, gate, upper, lower):
+        g = jnp.dot(rows, gate[...], preferred_element_type=jnp.float32)
+        u = jnp.dot(rows, upper[...], preferred_element_type=jnp.float32)
+        hidden = (g / (1.0 + jnp.exp(-g)) * u).astype(jnp.bfloat16)
+        return jnp.dot(hidden, lower[...], preferred_element_type=jnp.float32)
+
+    def expert(group):
+        for i in group:
+            pieces_in(i, ARR, arecv)
+        rows = jnp.concatenate(
+            [ARR[i, p].astype(jnp.float32) for i in group for p in range(8)], axis=0
+        ).astype(jnp.bfloat16)
+        done = gated(rows, wg, wu, wd)
+        for n, i in enumerate(group):
+            for p in range(8):
+                lo = (n * 8 + p) * CAP
+                EO[i, p] = done[lo : lo + CAP].astype(jnp.bfloat16)
+            pieces(i, EO, RET, rsend, rrecv)
+
+    def combine(i):
+        pieces_in(i, RET, rrecv)
+        hit, tab = matches(i)
+        share = jnp.zeros((64, 64), jnp.float32)
+        for k in range(4):
+            share = share + jnp.where(hit[k], tab[4 + k : 5 + k, 0:64], 0.0)
+        hi = share.astype(jnp.bfloat16)
+        lo = (share - hi.astype(jnp.float32)).astype(jnp.bfloat16)
+        back = jnp.concatenate(
+            [RET[i, p].astype(jnp.float32) for p in range(8)], axis=0
+        ).astype(jnp.bfloat16)
+        dims = (((0,), (0,)), ((), ()))
+        total = lax.dot_general(hi, back, dims, preferred_element_type=jnp.float32)
+        total = total + lax.dot_general(lo, back, dims, preferred_element_type=jnp.float32)
+        PART[i] = total.astype(jnp.bfloat16)
+
+    groups = ((0,), (1, 2), (3, 4), (5, 6), (7,))
+    for s in range(7):
+        if s < 5:
+            for i in groups[s]:
+                arrive(i)
+        if s == 0:
+            for w in weights[:3]:
+                w.wait()
+            out_ref[...] = (
+                hid_ref[...].astype(jnp.float32)
+                + gated(norm_ref[...], sg, su, sd).astype(jnp.bfloat16).astype(jnp.float32)
+            )
+            for w in weights[3:]:
+                w.wait()
+        if 0 <= s - 1 < 5:
+            expert(groups[s - 1])
+        if 0 <= s - 2 < 5:
+            for i in groups[s - 2]:
+                combine(i)
+
+    def back_z(src, dst, n, dev):
+        return pltpu.make_async_remote_copy(
+            src_ref=src, dst_ref=dst.at[n], send_sem=dsend.at[0 if dst is RD else 1, n],
+            recv_sem=drecv.at[0 if dst is RD else 1, n], device_id=dev, device_id_type=MESH_ID,
+        )
+
+    start(back_z(PART.at[at[-4]], RD, 3, down))
+    start(back_z(PART.at[at[3]], RU, 2, up))
+    for k in (3, 2, 1):
+        copy = back_z(PART.at[at[-k]], RD, k, down)
+        copy.wait_recv()
+        PART[at[-k]] = (
+            PART[at[-k]].astype(jnp.float32) + RD[k].astype(jnp.float32)
+        ).astype(jnp.bfloat16)
+        start(back_z(PART.at[at[-k]], RD, k - 1, down))
+        if k < 3:
+            back_z(PART.at[at[k]], RU, k, up).wait_recv()
+            PART[at[k]] = (
+                PART[at[k]].astype(jnp.float32) + RU[k].astype(jnp.float32)
+            ).astype(jnp.bfloat16)
+            start(back_z(PART.at[at[k]], RU, k - 1, up))
+    back_z(PART.at[0], RD, 0, down).wait_recv()
+    back_z(PART.at[0], RU, 0, up).wait_recv()
+    routed = PART[0].astype(jnp.float32) + RD[0].astype(jnp.float32) + RU[0].astype(jnp.float32)
+    out_ref[...] = out_ref[...] + routed.astype(jnp.bfloat16).astype(jnp.float32)
+
+    for copy in sends:
+        copy.wait_send()
+    for i in range(8):
+        pieces_sent(i, OUT, asend)
+        pieces_sent(i, EO, rsend)
+
+
+def experts_layer(normed, hidden, tables, wg, wu, wd, sg, su, sd):
+    vmem = pl.BlockSpec(memory_space=pltpu.VMEM)
+    hbm = pl.BlockSpec(memory_space=pl.ANY)
+    d, f = wg.shape
+    bf = jnp.bfloat16
+    return pl.pallas_call(
+        moe_kernel,
+        out_shape=jax.ShapeDtypeStruct((64, d), jnp.float32),
+        in_specs=[vmem] * 3 + [hbm] * 6,
+        out_specs=vmem,
+        scratch_shapes=[
+            pltpu.VMEM((8, 64, d), bf),
+            pltpu.VMEM((8, 8, CAP, d), bf),
+            pltpu.VMEM((8, 8, CAP, d), bf),
+            pltpu.VMEM((8, 8, CAP, d), bf),
+            pltpu.VMEM((8, 8, CAP, d), bf),
+            pltpu.VMEM((8, 64, d), bf),
+            pltpu.VMEM((4, 64, d), bf),
+            pltpu.VMEM((3, 64, d), bf),
+            pltpu.VMEM((d, f), bf),
+            pltpu.VMEM((d, f), bf),
+            pltpu.VMEM((f, d), bf),
+            pltpu.VMEM((d, f), bf),
+            pltpu.VMEM((d, f), bf),
+            pltpu.VMEM((f, d), bf),
+            pltpu.SemaphoreType.DMA((8,)),
+            pltpu.SemaphoreType.DMA((8,)),
+            pltpu.SemaphoreType.DMA((8,)),
+            pltpu.SemaphoreType.DMA((8,)),
+            pltpu.SemaphoreType.DMA((8,)),
+            pltpu.SemaphoreType.DMA((8,)),
+            pltpu.SemaphoreType.DMA((2, 4)),
+            pltpu.SemaphoreType.DMA((2, 4)),
+            pltpu.SemaphoreType.DMA((3,)),
+            pltpu.SemaphoreType.DMA((6,)),
+        ],
+        compiler_params=pltpu.CompilerParams(
+            collective_id=1, has_side_effects=True, vmem_limit_bytes=48 * 1024 * 1024
+        ),
+    )(normed, hidden, tables, wg, wu, wd, sg, su, sd)
+
+
 def body(
     query_nope,
     query_rope,
@@ -350,58 +565,17 @@
     tables = jnp.concatenate([expert_ids.astype(jnp.float32) * CAP + rank, route_weights], axis=1)
     tables = jnp.concatenate([tables.T, jnp.zeros((8, 64), jnp.float32)], axis=1)
     heads_out, gathered = gather_attend(payload, tables, q_cat, key_local, value_local)
-    tables = gathered[:, :, :64].transpose(0, 2, 1)
-    slot_of = tables[:, :, :4] - (z * 64).astype(jnp.float32)
-    weight_of = tables[:, :, 4:]
-    slots = jnp.arange(64, dtype=jnp.float32)
-    hit = slot_of[:, :, :, None] == slots
-    pick = jnp.any(hit, axis=2).astype(jnp.bfloat16)
-    share = jnp.sum(jnp.where(hit, weight_of[:, :, :, None], 0.0), axis=2)
-    share_hi = share.astype(jnp.bfloat16)
-    share_lo = (share - share_hi.astype(jnp.float32)).astype(jnp.bfloat16)
-
     part = jnp.dot(heads_out, out_proj, preferred_element_type=jnp.float32).astype(jnp.bfloat16)
     pieces = lax.all_to_all(part.reshape(4, 64, 2048), "y", 0, 0, tiled=True)
     attn_sum = jnp.sum(pieces.astype(jnp.float32), axis=0)
     hidden_one = (residual.astype(jnp.float32) + attn_sum).astype(jnp.bfloat16)
     normed = scale_rows(hidden_one, ffn_gain)
 
-    column = lax.all_gather(normed, "z", axis=0, tiled=False)
-    outgoing = jnp.einsum(
-        "stk,std->skd", pick, column, preferred_element_type=jnp.float32
-    ).astype(jnp.bfloat16)
-    outgoing = outgoing.reshape(8, 8, CAP, 2048).transpose(1, 0, 2, 3)
-    arrived = lax.all_to_all(outgoing, ("x", "core"), split_axis=0, concat_axis=0, tiled=True)
-    grouped = arrived.reshape(512, 2048)
-    gate_part = jnp.dot(grouped, expert_gate[0], preferred_element_type=jnp.float32)
-    upper_part = jnp.dot(grouped, expert_up[0], preferred_element_type=jnp.float32)
-    expert_hidden = (jax.nn.silu(gate_part) * upper_part).astype(jnp.bfloat16)
-    expert_rows = jnp.dot(
-        expert_hidden, expert_down[0], preferred_element_type=jnp.float32
-    ).astype(jnp.bfloat16)
-    returned = lax.all_to_all(
-        expert_rows.reshape(8, 8, CAP, 2048), ("x", "core"), split_axis=0, concat_axis=0, tiled=True
+    summed = experts_layer(
+        normed, hidden_one, gathered, expert_gate[0], expert_up[0], expert_down[0],
+        shared_gate, shared_up, shared_down,
     )
-    back = returned.transpose(1, 0, 2, 3).reshape(8, 64, 2048)
-    partial = jnp.einsum("stk,skd->std", share_hi, back, preferred_element_type=jnp.float32)
-    partial = partial + jnp.einsum(
-        "stk,skd->std", share_lo, back, preferred_element_type=jnp.float32
-    )
-    routed = lax.psum_scatter(
-        partial.astype(jnp.bfloat16), "z", scatter_dimension=0, tiled=False
-    )
-
-    shared_gate_part = jnp.dot(normed, shared_gate, preferred_element_type=jnp.float32)
-    shared_upper = jnp.dot(normed, shared_up, preferred_element_type=jnp.float32)
-    shared_hidden = (jax.nn.silu(shared_gate_part) * shared_upper).astype(jnp.bfloat16)
-    shared_rows = jnp.dot(shared_hidden, shared_down, preferred_element_type=jnp.float32).astype(
-        jnp.bfloat16
-    )
-    return (
-        hidden_one.astype(jnp.float32)
-        + routed.astype(jnp.float32)
-        + shared_rows.astype(jnp.float32)
-    ).astype(jnp.bfloat16)
+    return summed.astype(jnp.bfloat16)
 
 
 def solution(mesh):

time: 268 us -> 181 us (0.68)
  the two profiles are of different devices: /device:TPU:1 before, /device:TPU:6 now
where the time goes in v3:
time: 181 us
  Pallas kernels  148 us (82%)
  waiting for transfers between devices  16 us (9%)
  local copies, waits for them, and re-layouts  5.89 us (3%)
  starting transfers between devices  5.59 us (3%)
  other arithmetic  3.93 us (2%)
    pallas_call x1, Pallas kernels, experts_layer(): pl.pallas_call(moe_kernel, out_shape=jax.ShapeDtypeStruct((64, d), jnp.fl...  97.8 us
    pallas_call x1, Pallas kernels, gather_attend(): pl.pallas_call(gather_attend_kernel, out_shape=(jax.ShapeDtypeStruct((ROW...  49.9 us
    all_to_all x1, waiting for transfers between devices, body(): pieces = lax.all_to_all(part.reshape(4, 64, 2048), 'y', 0, 0, tiled=True)  16 us
    all_to_all x1, starting transfers between devices, body(): pieces = lax.all_to_all(part.reshape(4, 64, 2048), 'y', 0, 0, tiled=True)  5.59 us
    unnamed x27, local copies, waits for them, and re-layouts  3.82 us
  transfers between devices with their start and end apart: 1, of which 1 were waited for; matrix products, arithmetic and copies ran while one was open for 0% of the time, Pallas kernels for 0%

profile of v3, /device:TPU:6, one launch (start us, length us, event | category | flops | bytes accessed | tf_op | source)
XLA Modules:
  0.0 181.1 jit_solution(4274086207860651835)
XLA Ops:
  0.1 1.0 copy.26
  1.1 0.1 copy.30
  1.3 0.1 copy.31
  1.4 1.0 copy.25
  2.4 0.1 copy.29
  2.6 0.5 multiply_cosine_fusion
  3.1 0.2 fusion.12
  3.3 0.1 concatenate.26
  3.4 0.1 copy.21
  3.5 0.1 concatenate.27
  3.6 0.1 copy.22
  3.8 0.1 maximum_bitcast_fusion.1
  3.9 0.1 reshape.168
  4.0 0.1 fusion.4
  4.2 0.1 copy.23
  4.3 0.1 eq.15
  4.4 0.2 fusion
  4.6 0.1 reshape.169
  4.8 0.1 pad.4.clone
  4.9 0.1 fusion.6
  5.1 1.0 constant_dynamic-slice_fusion
  6.1 0.1 maximum_bitcast_fusion.q_ref
  6.3 49.9 %shard_map.172 = (bf16[256,256]{1,0:T(8,128)(2,1)S(1)}, f32[8,8,128]{2,1,0:T(8,128)S(1)}) custom-call(bf16[2,160,256]{2,1,0:T(8,128)(2,1)S(1)} %pad_maximum_fusion.pay_ref, f32[8,128]{1,0:T(8,128)S(1)} %concatenate.31.tab_ref, bf16[2,256,256]{2,1,0:T(8,128)(2,1)S(1)} %maximum_bitcast_fusion.q_ref, bf16[256,256]{1,0:T(8,128)(2,1)S(1)} %get-tuple-element.20.ku_ref, ...), custom_call_target="tpu_custom_call" | custom-call | tf_op jit(solution)/shard_map/pallas_call | solution.py:271
  56.1 1.5 convolution_convert_fusion
  57.6 5.6 %all-to-all-start = ((bf16[4,64,2048]{2,1,0:T(8,128)(2,1)}), bf16[4,64,2048]{2,1,0:T(8,128)(2,1)}, u32[]{:S(2)}, u32[]{:S(2)}) async-start(bf16[4,64,2048]{2,1,0:T(8,128)(2,1)} %bitcast.9), calls=%async_computation | async-start | bytes 2097152 | tf_op jit(solution)/shard_map/all_to_all | solution.py:569
  63.2 16.0 %all-to-all-done = bf16[4,64,2048]{2,1,0:T(8,128)(2,1)} async-done(((bf16[4,64,2048]{2,1,0:T(8,128)(2,1)}), bf16[4,64,2048]{2,1,0:T(8,128)(2,1)}, u32[]{:S(2)}, u32[]{:S(2)}) %all-to-all-start) | async-done | bytes 1048608 | tf_op jit(solution)/shard_map/all_to_all | solution.py:569
  79.2 1.5 convert_reduce_fusion
  80.8 0.2 fusion.1
  81.0 0.1 fusion.3.norm_ref
  81.2 1.4 copy-done.3
  82.6 97.8 %shard_map.173 = f32[64,2048]{1,0:T(8,128)S(1)} custom-call(bf16[64,2048]{1,0:T(8,128)(2,1)S(1)} %fusion.3.norm_ref, bf16[64,2048]{1,0:T(8,128)(2,1)S(1)} %get-tuple-element.10.hid_ref, f32[8,8,128]{2,1,0:T(8,128)S(1)} %get-tuple-element.8.tab_ref, bf16[2048,384]{1,0:T(8,128)(2,1)S(1)} %bitcast.23, bf16[2048,384]{1,0:T(8,128)(2,1)S(1)} %bitcast.24, ...), custom_call_target="tpu_custom_call" | custom-call | tf_op jit(solution)/shard_map/pallas_call | solution.py:479
  180.4 0.7 convert_element_type.79
  (36 shorter events, 0.3 us)
Async XLA Ops:
  0.0 56.1 %copy-start = (bf16[256,2048]{1,0:T(8,128)(2,1)S(1)}, bf16[256,2048]{1,0:T(8,128)(2,1)}, u32[]{:S(2)}) copy-start(bf16[256,2048]{1,0:T(8,128)(2,1)} %param.25) | copy-start | bytes 3145732
  0.0 2.5 %copy-start.6 = (bf16[256,64]{0,1:T(8,128)(2,1)S(1)}, bf16[256,64]{0,1:T(8,128)(2,1)}, u32[]{:S(2)}) copy-start(bf16[256,64]{0,1:T(8,128)(2,1)} %param.21) | copy-start | bytes 98308
  0.0 4.0 %copy-start.4 = (bf16[256,256]{1,0:T(8,128)(2,1)S(1)}, bf16[256,256]{1,0:T(8,128)(2,1)}, u32[]{:S(2)}) copy-start(bf16[256,256]{1,0:T(8,128)(2,1)} %param.20) | copy-start | bytes 393220
  0.0 4.1 %copy-start.10 = (bf16[256]{0:T(256)(128)(2,1)S(1)}, bf16[256]{0:T(256)(128)(2,1)}, u32[]{:S(2)}) copy-start(bf16[256]{0:T(256)(128)(2,1)} %param.22) | copy-start | bytes 1540
  0.0 4.2 %copy-start.7 = (s32[64,4]{0,1:T(4,128)S(1)}, s32[64,4]{0,1:T(4,128)}, u32[]{:S(2)}) copy-start(s32[64,4]{0,1:T(4,128)} %param.28) | copy-start | bytes 3076
  1.2 3.8 %copy-start.9 = (f32[64,4]{0,1:T(4,128)S(1)}, f32[64,4]{0,1:T(4,128)}, u32[]{:S(2)}) copy-start(f32[64,4]{0,1:T(4,128)} %param.29) | copy-start | bytes 3076
  57.6 5.6 %copy-start.8 = (bf16[2048]{0:T(1024)(128)(2,1)S(1)}, bf16[2048]{0:T(1024)(128)(2,1)}, u32[]{:S(2)}) copy-start(bf16[2048]{0:T(1024)(128)(2,1)} %param.27) | copy-start | bytes 12292
  57.6 23.2 %copy-start.5 = (bf16[64,2048]{1,0:T(8,128)(2,1)S(1)}, bf16[64,2048]{1,0:T(8,128)(2,1)}, u32[]{:S(2)}) copy-start(bf16[64,2048]{1,0:T(8,128)(2,1)} %param.26) | copy-start | bytes 786436
  57.6 21.6 %all-to-all-start = ((bf16[4,64,2048]{2,1,0:T(8,128)(2,1)}), bf16[4,64,2048]{2,1,0:T(8,128)(2,1)}, u32[]{:S(2)}, u32[]{:S(2)}) async-start(bf16[4,64,2048]{2,1,0:T(8,128)(2,1)} %bitcast.9), calls=%async_computation | async-start | bytes 2097152 | tf_op jit(solution)/shard_map/all_to_all | solution.py:569
  63.2 17.9 %copy-start.1 = (bf16[1,2048,384]{2,1,0:T(8,128)(2,1)S(1)}, bf16[1,2048,384]{2,1,0:T(8,128)(2,1)}, u32[]{:S(2)}) copy-start(bf16[1,2048,384]{2,1,0:T(8,128)(2,1)} %param.30) | copy-start | bytes 4718596
  79.2 1.9 %copy-start.2 = (bf16[1,2048,384]{2,1,0:T(8,128)(2,1)S(1)}, bf16[1,2048,384]{2,1,0:T(8,128)(2,1)}, u32[]{:S(2)}) copy-start(bf16[1,2048,384]{2,1,0:T(8,128)(2,1)} %param.31) | copy-start | bytes 4718596
  81.2 1.4 copy-start.3

commit v4 on v3

--- a/solution.py
+++ b/solution.py
@@ -44,6 +44,8 @@
 
 LOG2E = 1.4426950408889634
 MESH_ID = pl.DeviceIdType.MESH
+SUBS = 4
+WIDE = 512
 OFFS = (0, -1, 1, -2, 2, -3, 3, -4)
 HALF = 160
 
@@ -60,8 +62,10 @@
 
 
 def gather_attend_kernel(
-    pay_ref, tab_ref, q_ref, ku_ref, vu_ref, out_ref, tabs_ref,
-    G, T, m_ref, l_ref, acc_ref, recv, trecv, zsend, tsend, xsend, fsend, ysend, csend, lsem,
+    pay_ref, tab_ref, q_ref, ku_ref, vu_ref, op_ref, res_ref, fg_ref, hid_ref, norm_ref, tabs_ref,
+    G, T, m_ref, l_ref, acc_ref, W, HS, HX,
+    recv, trecv, zsend, tsend, xsend, fsend, ysend, csend, lsem,
+    wrecv, wsend, wfsend, wcsend, hrecv, hsend,
 ):
     z, x, c, y = (lax.axis_index(n) for n in ("z", "x", "core", "y"))
     hm = lax.rem(y, 2)
@@ -154,6 +158,52 @@
         arrived(c, zz, xs[dx], ho)
         to_mate(zz, xs[dx], ho)
 
+    yb, ya, y2 = ring(y - 1, NY), ring(y + 1, NY), ring(y + 2, NY)
+
+    def proj(yy, r, sem, dev):
+        slot = W.at[yy, c, r]
+        return pltpu.make_async_remote_copy(
+            src_ref=slot, dst_ref=slot, send_sem=sem, recv_sem=wrecv.at[yy, c, r],
+            device_id=dev, device_id_type=MESH_ID,
+        )
+
+    def proj_in(yy, half, r):
+        slot = W.at[yy, half, r]
+        pltpu.make_async_remote_copy(
+            src_ref=slot, dst_ref=slot, send_sem=wcsend, recv_sem=wrecv.at[yy, half, r],
+            device_id=mate, device_id_type=MESH_ID,
+        ).wait_recv()
+
+    def proj_send(yy, r, sems, where, dev):
+        proj(yy, r, sems.at[where], dev).start()
+        sent.append(lambda: proj(yy, r, sems.at[where], dev).wait_send())
+
+    def ev_proj(r):
+        proj_send(y, r, wsend, (0, r), above)
+        proj_send(y, r, wsend, (1, r), below)
+
+    def ev_proj1(r):
+        proj_in(yb, c, r)
+        if r % 2 == 0:
+            proj_send(yb, r, wfsend, (r,), above)
+        proj(yb, r, wcsend, mate).start()
+        proj_in(ya, c, r)
+        if r % 2 == 1:
+            proj_send(ya, r, wfsend, (r,), below)
+        proj(ya, r, wcsend, mate).start()
+
+    def ev_proj2(r):
+        proj_in(y2, c, r)
+        proj(y2, r, wcsend, mate).start()
+
+    own_proj = [
+        pltpu.make_async_copy(
+            op_ref.at[:, :, half * 1024 : (half + 1) * 1024], W.at[y, half], lsem.at[2 + half]
+        )
+        for half in range(2)
+    ]
+    for copy in own_proj:
+        copy.start()
     own = pltpu.make_async_copy(pay_ref, G.at[c, z, x], lsem.at[0])
     own_table = pltpu.make_async_copy(tab_ref, T.at[z], lsem.at[1])
     own.start()
@@ -226,6 +276,15 @@
                     ev_y(k - 2, 1)
                 if 0 <= k - 3 < 8:
                     ev_y(k - 3, 2)
+                if k == 1:
+                    for copy in own_proj:
+                        copy.wait()
+                if 0 <= k - 1 < 8:
+                    ev_proj(k - 1)
+                if 0 <= k - 2 < 8:
+                    ev_proj1(k - 2)
+                if 0 <= k - 3 < 8:
+                    ev_proj2(k - 3)
 
         def pair(d, carry):
             i = s - 1 - jnp.where(d == 0, 0, jnp.where(d == 3, 3, 2))
@@ -255,8 +314,50 @@
     lax.fori_loop(0, 12, round_, 0)
 
     for h in range(2):
-        out_ref[:, h * VDIM : (h + 1) * VDIM] = (acc_ref[h] / l_ref[h]).astype(jnp.bfloat16)
+        heads = (acc_ref[h] / l_ref[h]).astype(jnp.bfloat16)
+        for q in range(NY):
+            HS[q, :, h * VDIM : (h + 1) * VDIM] = heads[q * 64 : (q + 1) * 64]
+
+    def heads_to(yy):
+        return pltpu.make_async_remote_copy(
+            src_ref=HS.at[yy], dst_ref=HX.at[y], send_sem=hsend.at[yy], recv_sem=hrecv.at[y],
+            device_id={"y": yy}, device_id_type=MESH_ID,
+        )
+
+    for yy in (y2, ya, yb):
+        heads_to(yy).start()
+    HX[y] = HS[y]
     tabs_ref[...] = T[...]
+    for yy in (yb, ya, y2):
+        for r in range(8):
+            proj_in(yy, 1 - c, r)
+    for yy in (yb, ya, y2):
+        pltpu.make_async_remote_copy(
+            src_ref=HS.at[yy], dst_ref=HX.at[yy], send_sem=hsend.at[yy], recv_sem=hrecv.at[yy],
+            device_id={"y": yy}, device_id_type=MESH_ID,
+        ).wait_recv()
+    squares = jnp.zeros((64, 1), jnp.float32)
+    for half in range(2):
+        lanes = slice(half * 1024, (half + 1) * 1024)
+        total = jnp.zeros((64, 1024), jnp.float32)
+        for q in range(NY):
+            weight = jnp.concatenate([W[q, half, r] for r in range(8)], axis=0)
+            rows = jnp.dot(HX[q], weight, preferred_element_type=jnp.float32)
+            total = total + rows.astype(jnp.bfloat16).astype(jnp.float32)
+        one = (res_ref[:, lanes].astype(jnp.float32) + total).astype(jnp.bfloat16)
+        hid_ref[:, lanes] = one
+        one = one.astype(jnp.float32)
+        squares = squares + jnp.sum(one * one, axis=1, keepdims=True)
+    factor = lax.rsqrt(squares * (1.0 / 2048) + norm_eps)
+    norm_ref[...] = (
+        hid_ref[...].astype(jnp.float32) * factor * fg_ref[...].astype(jnp.float32)
+    ).astype(jnp.bfloat16)
+    for yy in (y2, ya, yb):
+        heads_to(yy).wait_send()
+    pltpu.make_async_remote_copy(
+        src_ref=W.at[0:3, 0], dst_ref=W.at[0:3, 0], send_sem=wcsend, recv_sem=wrecv.at[0, 0, 0],
+        device_id=mate, device_id_type=MESH_ID,
+    ).wait_send()
     for wait in sent:
         wait()
     whole = G.at[c]
@@ -266,22 +367,27 @@
     ).wait_send()
 
 
-def gather_attend(payload, tables, q_cat, key_local, value_local):
+def gather_attend(payload, tables, q_cat, key_local, value_local, out_proj, residual, gain):
     vmem = pl.BlockSpec(memory_space=pltpu.VMEM)
+    hbm = pl.BlockSpec(memory_space=pl.ANY)
     return pl.pallas_call(
         gather_attend_kernel,
         out_shape=(
-            jax.ShapeDtypeStruct((ROWS, 256), jnp.bfloat16),
+            jax.ShapeDtypeStruct((64, 2048), jnp.bfloat16),
+            jax.ShapeDtypeStruct((64, 2048), jnp.bfloat16),
             jax.ShapeDtypeStruct((NZ, 8, 128), jnp.float32),
         ),
-        in_specs=[vmem] * 5,
-        out_specs=(vmem, vmem),
+        in_specs=[vmem] * 5 + [hbm, vmem, vmem],
+        out_specs=(vmem, vmem, vmem),
         scratch_shapes=[
             pltpu.VMEM((2, NZ, NX, 2, HALF, 256), jnp.bfloat16),
             pltpu.VMEM((NZ, 8, 128), jnp.float32),
             pltpu.VMEM((2, ROWS, 128), jnp.float32),
             pltpu.VMEM((2, ROWS, 128), jnp.float32),
             pltpu.VMEM((2, ROWS, 128), jnp.float32),
+            pltpu.VMEM((NY, 2, 8, 32, 1024), jnp.bfloat16),
+            pltpu.VMEM((NY, 64, 256), jnp.bfloat16),
+            pltpu.VMEM((NY, 64, 256), jnp.bfloat16),
             pltpu.SemaphoreType.DMA((2, NZ, NX, 2)),
             pltpu.SemaphoreType.DMA((NZ,)),
             pltpu.SemaphoreType.DMA((2, 4, 2)),
@@ -290,12 +396,21 @@
             pltpu.SemaphoreType.DMA((8,)),
             pltpu.SemaphoreType.DMA((8, 3)),
             pltpu.SemaphoreType.DMA,
-            pltpu.SemaphoreType.DMA((2,)),
+            pltpu.SemaphoreType.DMA((4,)),
+            pltpu.SemaphoreType.DMA((NY, 2, 8)),
+            pltpu.SemaphoreType.DMA((2, 8)),
+            pltpu.SemaphoreType.DMA((8,)),
+            pltpu.SemaphoreType.DMA,
+            pltpu.SemaphoreType.DMA((NY,)),
+            pltpu.SemaphoreType.DMA((NY,)),
         ],
         compiler_params=pltpu.CompilerParams(
-            collective_id=0, has_side_effects=True, vmem_limit_bytes=40 * 1024 * 1024
+            collective_id=0, has_side_effects=True, vmem_limit_bytes=63 * 1024 * 1024
         ),
-    )(payload, tables, q_cat, key_local, value_local)
+    )(
+        payload, tables, q_cat, key_local, value_local, out_proj.reshape(8, 32, 2048), residual,
+        gain.reshape(1, 2048),
+    )
 
 
 def moe_kernel(
@@ -317,20 +432,31 @@
             ((sg_h, sg), (su_h, su), (sd_h, sd), (wg_h, wg), (wu_h, wu), (wd_h, wd))
         )
     ]
-    own = pltpu.make_async_copy(norm_ref, COL.at[0], lsem.at[0])
-    own.start()
+    for b in range(SUBS):
+        COL[0, b] = norm_ref[:, b * WIDE : (b + 1) * WIDE]
     for w in weights:
         w.start()
     greet([up, down] + [dev for _, dev in peers])
-    own.wait()
 
     at = {off: i for i, off in enumerate(OFFS)}
 
-    def along_z(i, dev, off_to, sems, n):
+    def along_z(i, b, dev, off_to, n):
+        there = at[off_to]
         return pltpu.make_async_remote_copy(
-            src_ref=COL.at[i], dst_ref=COL.at[at[off_to]], send_sem=sems.at[n],
-            recv_sem=zrecv.at[at[off_to]], device_id=dev, device_id_type=MESH_ID,
-        )
+            src_ref=COL.at[i, b], dst_ref=COL.at[there, b], send_sem=zsend.at[n, b],
+            recv_sem=zrecv.at[there, b], device_id=dev, device_id_type=MESH_ID,
+        )
+
+    def pass_on(off, b):
+        i = at[off]
+        if off != 0:
+            along_z(i, b, up, off, 0).wait_recv()
+        if -3 < off <= 0 or (off == -3 and b < 2):
+            start(along_z(i, b, up, off - 1, -off))
+        if 0 <= off < 3:
+            start(along_z(i, b, down, off + 1, 4 + off))
+        if off == 3 and b >= 2:
+            start(along_z(i, b, down, -4, 7))
 
     sends = []
 
@@ -368,20 +494,16 @@
         base = (z * 64).astype(jnp.float32)
         return [(tab[k : k + 1, 0:64] - base) == slots for k in range(4)], tab
 
-    def arrive(i):
-        off = OFFS[i]
-        if i > 0:
-            along_z(i, up, off, zsend, 0).wait_recv()
-        if -4 < off <= 0:
-            start(along_z(i, up, off - 1, zsend, -off))
-        if 0 <= off < 3:
-            start(along_z(i, down, off + 1, zsend, 4 + off))
+    def picks(i):
         hit, _ = matches(i)
-        pick = jnp.where(hit[0] | hit[1] | hit[2] | hit[3], 1.0, 0.0).astype(jnp.bfloat16)
-        rows = jnp.dot(pick, COL[i], preferred_element_type=jnp.float32)
+        return jnp.where(hit[0] | hit[1] | hit[2] | hit[3], 1.0, 0.0).astype(jnp.bfloat16)
+
+    def select(i, b, pick):
+        rows = jnp.dot(pick, COL[i, b], preferred_element_type=jnp.float32)
         for p in range(8):
-            OUT[i, p] = rows[p * CAP : (p + 1) * CAP].astype(jnp.bfloat16)
-        pieces(i, OUT, ARR, asend, arecv)
+            OUT[i, p, :, b * WIDE : (b + 1) * WIDE] = rows[p * CAP : (p + 1) * CAP].astype(
+                jnp.bfloat16
+            )
 
     def gated(rows, gate, upper, lower):
         g = jnp.dot(rows, gate[...], preferred_element_type=jnp.float32)
@@ -416,53 +538,90 @@
         dims = (((0,), (0,)), ((), ()))
         total = lax.dot_general(hi, back, dims, preferred_element_type=jnp.float32)
         total = total + lax.dot_general(lo, back, dims, preferred_element_type=jnp.float32)
-        PART[i] = total.astype(jnp.bfloat16)
+        for b in range(SUBS):
+            PART[i, b] = total[:, b * WIDE : (b + 1) * WIDE].astype(jnp.bfloat16)
 
     groups = ((0,), (1, 2), (3, 4), (5, 6), (7,))
-    for s in range(7):
-        if s < 5:
-            for i in groups[s]:
-                arrive(i)
-        if s == 0:
-            for w in weights[:3]:
-                w.wait()
-            out_ref[...] = (
-                hid_ref[...].astype(jnp.float32)
-                + gated(norm_ref[...], sg, su, sd).astype(jnp.bfloat16).astype(jnp.float32)
-            )
-            for w in weights[3:]:
-                w.wait()
-        if 0 <= s - 1 < 5:
-            expert(groups[s - 1])
-        if 0 <= s - 2 < 5:
-            for i in groups[s - 2]:
-                combine(i)
-
-    def back_z(src, dst, n, dev):
+
+    def shared():
+        for w in weights[:3]:
+            w.wait()
+        rows = jnp.concatenate([COL[0, b] for b in range(SUBS)], axis=1)
+        out_ref[...] = (
+            hid_ref[...].astype(jnp.float32)
+            + gated(rows, sg, su, sd).astype(jnp.bfloat16).astype(jnp.float32)
+        )
+
+    def between(s, b):
+        if s == 1 and b == 3:
+            shared()
+        if s >= 2 and b == 1:
+            if s == 2:
+                for w in weights[3:]:
+                    w.wait()
+            expert(groups[s - 2])
+        if s >= 3 and b >= 2 and b - 2 < len(groups[s - 3]):
+            combine(groups[s - 3][b - 2])
+
+    for s in range(5):
+        pick = [picks(i) for i in groups[s]]
+        for b in range(SUBS):
+            for n, i in enumerate(groups[s]):
+                pass_on(OFFS[i], b)
+            for n, i in enumerate(groups[s]):
+                select(i, b, pick[n])
+            between(s, b)
+        for i in groups[s]:
+            pieces(i, OUT, ARR, asend, arecv)
+    expert(groups[3])
+    for i in groups[2]:
+        combine(i)
+    expert(groups[4])
+
+    def back_z(i, b, way, k):
+        dst, dev = ((RD, down), (RU, up))[way]
         return pltpu.make_async_remote_copy(
-            src_ref=src, dst_ref=dst.at[n], send_sem=dsend.at[0 if dst is RD else 1, n],
-            recv_sem=drecv.at[0 if dst is RD else 1, n], device_id=dev, device_id_type=MESH_ID,
-        )
-
-    start(back_z(PART.at[at[-4]], RD, 3, down))
-    start(back_z(PART.at[at[3]], RU, 2, up))
+            src_ref=PART.at[i, b], dst_ref=dst.at[k, b], send_sem=dsend.at[way, k, b],
+            recv_sem=drecv.at[way, k, b], device_id=dev, device_id_type=MESH_ID,
+        )
+
+    def chain(way, k, b):
+        i = at[-k if way == 0 or k == 4 else k]
+        if k < 3 or (k == 3 and (b < 2) == (way == 0)):
+            back_z(i, b, way, k).wait_recv()
+            dst = (RD, RU)[way]
+            PART[i, b] = (
+                PART[i, b].astype(jnp.float32) + dst[k, b].astype(jnp.float32)
+            ).astype(jnp.bfloat16)
+        start(back_z(i, b, way, k - 1))
+
+    combine(groups[3][0])
+    for b in (2, 3):
+        chain(0, 3, b)
+    combine(groups[3][1])
+    for b in (0, 1):
+        chain(1, 3, b)
+    combine(groups[4][0])
+    for n in range(2):
+        chain(0, 4, n)
+        chain(1, 4, n + 2)
     for k in (3, 2, 1):
-        copy = back_z(PART.at[at[-k]], RD, k, down)
-        copy.wait_recv()
-        PART[at[-k]] = (
-            PART[at[-k]].astype(jnp.float32) + RD[k].astype(jnp.float32)
-        ).astype(jnp.bfloat16)
-        start(back_z(PART.at[at[-k]], RD, k - 1, down))
-        if k < 3:
-            back_z(PART.at[at[k]], RU, k, up).wait_recv()
-            PART[at[k]] = (
-                PART[at[k]].astype(jnp.float32) + RU[k].astype(jnp.float32)
-            ).astype(jnp.bfloat16)
-            start(back_z(PART.at[at[k]], RU, k - 1, up))
-    back_z(PART.at[0], RD, 0, down).wait_recv()
-    back_z(PART.at[0], RU, 0, up).wait_recv()
-    routed = PART[0].astype(jnp.float32) + RD[0].astype(jnp.float32) + RU[0].astype(jnp.float32)
-    out_ref[...] = out_ref[...] + routed.astype(jnp.bfloat16).astype(jnp.float32)
+        for n in range(4):
+            down_b, up_b = (n + 2) % 4, n
+            if k < 3 or down_b < 2:
+                chain(0, k, down_b)
+            if k < 3 or up_b >= 2:
+                chain(1, k, up_b)
+    for n in range(4):
+        back_z(0, n, 0, 0).wait_recv()
+        back_z(0, n, 1, 0).wait_recv()
+        lanes = slice(n * WIDE, (n + 1) * WIDE)
+        routed = (
+            PART[0, n].astype(jnp.float32)
+            + RD[0, n].astype(jnp.float32)
+            + RU[0, n].astype(jnp.float32)
+        )
+        out_ref[:, lanes] = out_ref[:, lanes] + routed.astype(jnp.bfloat16).astype(jnp.float32)
 
     for copy in sends:
         copy.wait_send()
@@ -482,33 +641,33 @@
         in_specs=[vmem] * 3 + [hbm] * 6,
         out_specs=vmem,
         scratch_shapes=[
-            pltpu.VMEM((8, 64, d), bf),
+            pltpu.VMEM((8, SUBS, 64, WIDE), bf),
             pltpu.VMEM((8, 8, CAP, d), bf),
             pltpu.VMEM((8, 8, CAP, d), bf),
             pltpu.VMEM((8, 8, CAP, d), bf),
             pltpu.VMEM((8, 8, CAP, d), bf),
-            pltpu.VMEM((8, 64, d), bf),
-            pltpu.VMEM((4, 64, d), bf),
-            pltpu.VMEM((3, 64, d), bf),
+            pltpu.VMEM((8, SUBS, 64, WIDE), bf),
+            pltpu.VMEM((4, SUBS, 64, WIDE), bf),
+            pltpu.VMEM((4, SUBS, 64, WIDE), bf),
             pltpu.VMEM((d, f), bf),
             pltpu.VMEM((d, f), bf),
             pltpu.VMEM((f, d), bf),
             pltpu.VMEM((d, f), bf),
             pltpu.VMEM((d, f), bf),
             pltpu.VMEM((f, d), bf),
+            pltpu.SemaphoreType.DMA((8, SUBS)),
+            pltpu.SemaphoreType.DMA((8, SUBS)),
             pltpu.SemaphoreType.DMA((8,)),
             pltpu.SemaphoreType.DMA((8,)),
             pltpu.SemaphoreType.DMA((8,)),
             pltpu.SemaphoreType.DMA((8,)),
-            pltpu.SemaphoreType.DMA((8,)),
-            pltpu.SemaphoreType.DMA((8,)),
-            pltpu.SemaphoreType.DMA((2, 4)),
-            pltpu.SemaphoreType.DMA((2, 4)),
+            pltpu.SemaphoreType.DMA((2, 4, SUBS)),
+            pltpu.SemaphoreType.DMA((2, 4, SUBS)),
             pltpu.SemaphoreType.DMA((3,)),
             pltpu.SemaphoreType.DMA((6,)),
         ],
         compiler_params=pltpu.CompilerParams(
-            collective_id=1, has_side_effects=True, vmem_limit_bytes=48 * 1024 * 1024
+            collective_id=1, has_side_effects=True, vmem_limit_bytes=63 * 1024 * 1024
         ),
     )(normed, hidden, tables, wg, wu, wd, sg, su, sd)
 
@@ -564,13 +723,9 @@
     rank = jnp.sum(before * onehot, axis=1).reshape(64, 4)
     tables = jnp.concatenate([expert_ids.astype(jnp.float32) * CAP + rank, route_weights], axis=1)
     tables = jnp.concatenate([tables.T, jnp.zeros((8, 64), jnp.float32)], axis=1)
-    heads_out, gathered = gather_attend(payload, tables, q_cat, key_local, value_local)
-    part = jnp.dot(heads_out, out_proj, preferred_element_type=jnp.float32).astype(jnp.bfloat16)
-    pieces = lax.all_to_all(part.reshape(4, 64, 2048), "y", 0, 0, tiled=True)
-    attn_sum = jnp.sum(pieces.astype(jnp.float32), axis=0)
-    hidden_one = (residual.astype(jnp.float32) + attn_sum).astype(jnp.bfloat16)
-    normed = scale_rows(hidden_one, ffn_gain)
-
+    hidden_one, normed, gathered = gather_attend(
+        payload, tables, q_cat, key_local, value_local, out_proj, residual, ffn_gain
+    )
     summed = experts_layer(
         normed, hidden_one, gathered, expert_gate[0], expert_up[0], expert_down[0],
         shared_gate, shared_up, shared_down,

time: 181 us -> 172 us (0.950)
  the two profiles are of different devices: /device:TPU:6 before, /device:TPU:1 now
where the time goes in v4:
time: 172 us
  Pallas kernels  162 us (94%)
  local copies, waits for them, and re-layouts  5.36 us (3%)
  other arithmetic  4.44 us (3%)
    pallas_call x1, Pallas kernels, experts_layer(): pl.pallas_call(moe_kernel, out_shape=jax.ShapeDtypeStruct((64, d), jnp.fl...  95.1 us
    pallas_call x1, Pallas kernels, gather_attend(): pl.pallas_call(gather_attend_kernel, out_shape=(jax.ShapeDtypeStruct((64,...  66.5 us

profile of v4, /device:TPU:1, one launch (start us, length us, event | category | flops | bytes accessed | tf_op | source)
XLA Modules:
  0.0 171.9 jit_solution(14815817814917880528)
XLA Ops:
  0.0 0.5 multiply_cosine_fusion
  0.6 0.9 copy.26
  1.5 0.1 copy.30
  1.7 0.1 copy.31
  1.8 0.0 copy-start.6
  1.8 0.1 subtract_convert_fusion
  1.9 0.1 copy.25
  2.0 0.0 copy-start.3
  2.0 0.1 copy.29
  2.2 0.1 pad.4.clone
  2.3 0.8 maximum_bitcast_fusion.q_ref
  3.1 0.2 fusion.9
  3.3 0.1 concatenate.26
  3.4 0.1 copy.21
  3.5 0.1 concatenate.27
  3.6 0.1 copy.22
  3.8 0.1 maximum_bitcast_fusion.1
  3.9 0.1 reshape.162
  4.0 0.1 fusion.1
  4.2 0.1 fusion.3
  4.3 0.7 pad_maximum_fusion.pay_ref
  4.9 1.7 constant_dynamic-slice_fusion
  6.6 0.1 copy.23
  6.7 0.1 eq.15
  6.8 0.2 fusion
  7.0 0.1 reshape.163
  7.1 0.1 copy.24
  7.2 0.6 concatenate.31.tab_ref
  7.8 0.6 reshape.166.fg_ref
  8.4 66.5 %shard_map.172 = (bf16[64,2048]{1,0:T(8,128)(2,1)}, bf16[64,2048]{1,0:T(8,128)(2,1)}, f32[8,8,128]{2,1,0:T(8,128)}) custom-call(bf16[2,160,256]{2,1,0:T(8,128)(2,1)} %pad_maximum_fusion.pay_ref, f32[8,128]{1,0:T(8,128)} %concatenate.31.tab_ref, bf16[2,256,256]{2,1,0:T(8,128)(2,1)} %maximum_bitcast_fusion.q_ref, bf16[256,256]{1,0:T(8,128)(2,1)} %get-tuple-element.20.ku_ref, ...), custom_call_target="tpu_custom_call" | custom-call | tf_op jit(solution)/shard_map/pallas_call | solution.py:373
  75.0 95.1 %shard_map.173 = f32[64,2048]{1,0:T(8,128)} custom-call(bf16[64,2048]{1,0:T(8,128)(2,1)} %get-tuple-element.8.norm_ref, bf16[64,2048]{1,0:T(8,128)(2,1)} %get-tuple-element.9.hid_ref, f32[8,8,128]{2,1,0:T(8,128)} %get-tuple-element.10.tab_ref, bf16[2048,384]{1,0:T(8,128)(2,1)} %bitcast.21, bf16[2048,384]{1,0:T(8,128)(2,1)} %bitcast.22, ...), custom_call_target="tpu_custom_call" | custom-call | tf_op jit(solution)/shard_map/pallas_call | solution.py:638
  170.1 1.8 %convert_element_type.51 = bf16[64,2048]{1,0:T(8,128)(2,1)} convert(f32[64,2048]{1,0:T(8,128)} %shard_map.173) | non-fusion elementwise | flops 131072 | bytes 786432 | tf_op jit(solution)/shard_map/convert_element_type | solution.py:733
  (21 shorter events, 0.1 us)
Async XLA Ops:
  0.0 1.9 %copy-start.1 = (bf16[256,256]{1,0:T(8,128)(2,1)S(1)}, bf16[256,256]{1,0:T(8,128)(2,1)}, u32[]{:S(2)}) copy-start(bf16[256,256]{1,0:T(8,128)(2,1)} %param.18) | copy-start | bytes 393220
  1.5 1.6 copy-start.2
  1.8 2.2 %copy-start = (bf16[256,256]{1,0:T(8,128)(2,1)S(1)}, bf16[256,256]{1,0:T(8,128)(2,1)}, u32[]{:S(2)}) copy-start(bf16[256,256]{1,0:T(8,128)(2,1)} %param.20) | copy-start | bytes 393220
  1.8 2.3 %copy-start.6 = (bf16[256]{0:T(256)(128)(2,1)S(1)}, bf16[256]{0:T(256)(128)(2,1)}, u32[]{:S(2)}) copy-start(bf16[256]{0:T(256)(128)(2,1)} %param.22) | copy-start | bytes 1540
  2.0 4.6 %copy-start.3 = (s32[64,4]{0,1:T(4,128)S(1)}, s32[64,4]{0,1:T(4,128)}, u32[]{:S(2)}) copy-start(s32[64,4]{0,1:T(4,128)} %param.28) | copy-start | bytes 3076
  2.3 5.0 %copy-start.5 = (f32[64,4]{0,1:T(4,128)S(1)}, f32[64,4]{0,1:T(4,128)}, u32[]{:S(2)}) copy-start(f32[64,4]{0,1:T(4,128)} %param.29) | copy-start | bytes 3076
  2.3 5.6 %copy-start.4 = (bf16[2048]{0:T(1024)(128)(2,1)S(1)}, bf16[2048]{0:T(1024)(128)(2,1)}, u32[]{:S(2)}) copy-start(bf16[2048]{0:T(1024)(128)(2,1)} %param.27) | copy-start | bytes 12292

commit v5 on v4

--- a/solution.py
+++ b/solution.py
@@ -262,7 +262,7 @@
     mine = z * NX + x
 
     def round_(s, carry):
-        for k in range(11):
+        for k in range(13):
 
             @pl.when(s == k)
             def _():
@@ -272,22 +272,23 @@
                     ev_x1(k - 1)
                 if 0 <= k - 2 < 8:
                     ev_x2(k - 2)
-                    ev_y(k - 2, -1)
-                    ev_y(k - 2, 1)
                 if 0 <= k - 3 < 8:
-                    ev_y(k - 3, 2)
+                    ev_y(k - 3, -1)
+                    ev_y(k - 3, 1)
+                if 0 <= k - 4 < 8:
+                    ev_y(k - 4, 2)
                 if k == 1:
                     for copy in own_proj:
                         copy.wait()
                 if 0 <= k - 1 < 8:
                     ev_proj(k - 1)
-                if 0 <= k - 2 < 8:
-                    ev_proj1(k - 2)
                 if 0 <= k - 3 < 8:
-                    ev_proj2(k - 3)
+                    ev_proj1(k - 3)
+                if 0 <= k - 5 < 8:
+                    ev_proj2(k - 5)
 
         def pair(d, carry):
-            i = s - 1 - jnp.where(d == 0, 0, jnp.where(d == 3, 3, 2))
+            i = s - 1 - jnp.where(d == 0, 0, jnp.where(d == 3, 4, 3))
 
             @pl.when((i >= 0) & (i < 8))
             def _():
@@ -311,7 +312,7 @@
 
         return lax.fori_loop(0, 4, pair, carry)
 
-    lax.fori_loop(0, 12, round_, 0)
+    lax.fori_loop(0, 13, round_, 0)
 
     for h in range(2):
         heads = (acc_ref[h] / l_ref[h]).astype(jnp.bfloat16)
@@ -429,7 +430,7 @@
     weights = [
         pltpu.make_async_copy(src, dst, wsem.at[n])
         for n, (src, dst) in enumerate(
-            ((sg_h, sg), (su_h, su), (sd_h, sd), (wg_h, wg), (wu_h, wu), (wd_h, wd))
+            ((wg_h, wg), (wu_h, wu), (wd_h, wd), (sg_h, sg), (su_h, su), (sd_h, sd))
         )
     ]
     for b in range(SUBS):
@@ -522,7 +523,6 @@
             for p in range(8):
                 lo = (n * 8 + p) * CAP
                 EO[i, p] = done[lo : lo + CAP].astype(jnp.bfloat16)
-            pieces(i, EO, RET, rsend, rrecv)
 
     def combine(i):
         pieces_in(i, RET, rrecv)
@@ -544,7 +544,7 @@
     groups = ((0,), (1, 2), (3, 4), (5, 6), (7,))
 
     def shared():
-        for w in weights[:3]:
+        for w in weights[3:]:
             w.wait()
         rows = jnp.concatenate([COL[0, b] for b in range(SUBS)], axis=1)
         out_ref[...] = (
@@ -553,15 +553,11 @@
         )
 
     def between(s, b):
-        if s == 1 and b == 3:
-            shared()
         if s >= 2 and b == 1:
             if s == 2:
-                for w in weights[3:]:
+                for w in weights[:3]:
                     w.wait()
             expert(groups[s - 2])
-        if s >= 3 and b >= 2 and b - 2 < len(groups[s - 3]):
-            combine(groups[s - 3][b - 2])
 
     for s in range(5):
         pick = [picks(i) for i in groups[s]]
@@ -574,9 +570,11 @@
         for i in groups[s]:
             pieces(i, OUT, ARR, asend, arecv)
     expert(groups[3])
-    for i in groups[2]:
-        combine(i)
     expert(groups[4])
+    for group in reversed(groups):
+        for i in group:
+            pieces(i, EO, RET, rsend, rrecv)
+    shared()
 
     def back_z(i, b, way, k):
         dst, dev = ((RD, down), (RU, up))[way]
@@ -595,23 +593,17 @@
             ).astype(jnp.bfloat16)
         start(back_z(i, b, way, k - 1))
 
-    combine(groups[3][0])
-    for b in (2, 3):
-        chain(0, 3, b)
-    combine(groups[3][1])
-    for b in (0, 1):
-        chain(1, 3, b)
-    combine(groups[4][0])
+    combine(7)
     for n in range(2):
         chain(0, 4, n)
         chain(1, 4, n + 2)
     for k in (3, 2, 1):
+        for i in groups[k]:
+            combine(i)
         for n in range(4):
-            down_b, up_b = (n + 2) % 4, n
-            if k < 3 or down_b < 2:
-                chain(0, k, down_b)
-            if k < 3 or up_b >= 2:
-                chain(1, k, up_b)
+            chain(0, k, (n + 2) % 4)
+            chain(1, k, n)
+    combine(0)
     for n in range(4):
         back_z(0, n, 0, 0).wait_recv()
         back_z(0, n, 1, 0).wait_recv()

time: 172 us -> 153 us (0.89)
  Pallas kernels: 162 us -> 143 us
    pallas_call x1, Pallas kernels: 95.1 us -> 78.1 us  [experts_layer(): pl.pallas_call(moe_kernel, out_shape=jax.ShapeDtypeStruct((64, d), jnp.fl...]
    pallas_call x1, Pallas kernels: 66.5 us -> 64.5 us  [gather_attend(): pl.pallas_call(gather_attend_kernel, out_shape=(jax.ShapeDtypeStruct((64,...]
where the time goes in v5:
time: 153 us
  Pallas kernels  143 us (93%)
  local copies, waits for them, and re-layouts  5.36 us (4%)
  other arithmetic  4.44 us (3%)
    pallas_call x1, Pallas kernels, experts_layer(): pl.pallas_call(moe_kernel, out_shape=jax.ShapeDtypeStruct((64, d), jnp.fl...  78.1 us
    pallas_call x1, Pallas kernels, gather_attend(): pl.pallas_call(gather_attend_kernel, out_shape=(jax.ShapeDtypeStruct((64,...  64.5 us

profile of v5, /device:TPU:1, one launch (start us, length us, event | category | flops | bytes accessed | tf_op | source)
XLA Modules:
  0.0 152.8 jit_solution(12801944304053507461)
XLA Ops:
  0.0 0.5 multiply_cosine_fusion
  0.6 0.9 copy.26
  1.5 0.1 copy.30
  1.7 0.1 copy.31
  1.8 0.0 copy-start.6
  1.8 0.1 subtract_convert_fusion
  1.9 0.1 copy.25
  2.0 0.0 copy-start.3
  2.0 0.1 copy.29
  2.2 0.1 pad.4.clone
  2.3 0.8 maximum_bitcast_fusion.q_ref
  3.1 0.2 fusion.9
  3.3 0.1 concatenate.26
  3.4 0.1 copy.21
  3.5 0.1 concatenate.27
  3.6 0.1 copy.22
  3.8 0.1 maximum_bitcast_fusion.1
  3.9 0.1 reshape.162
  4.0 0.1 fusion.1
  4.2 0.1 fusion.3
  4.3 0.7 pad_maximum_fusion.pay_ref
  4.9 1.7 %constant_dynamic-slice_fusion = (bf16[256,256]{1,0:T(8,128)(2,1)}, bf16[256,256]{1,0:T(8,128)(2,1)}) fusion(bf16[256,1024]{1,0:T(8,128)(2,1)} %param.24, s32[]{:T(128)S(6)} %select_n.4, bf16[256,1024]{1,0:T(8,128)(2,1)} %param.23), kind=kLoop, calls=%fused_computation.32 | loop fusion | bytes 524292 | tf_op jit(solution)/shard_map/dynamic_slice | solution.py:698
  6.6 0.1 copy.23
  6.7 0.1 eq.15
  6.8 0.2 fusion
  7.0 0.1 reshape.163
  7.1 0.1 copy.24
  7.2 0.6 concatenate.31.tab_ref
  7.8 0.6 reshape.166.fg_ref
  8.4 64.5 %shard_map.172 = (bf16[64,2048]{1,0:T(8,128)(2,1)}, bf16[64,2048]{1,0:T(8,128)(2,1)}, f32[8,8,128]{2,1,0:T(8,128)}) custom-call(bf16[2,160,256]{2,1,0:T(8,128)(2,1)} %pad_maximum_fusion.pay_ref, f32[8,128]{1,0:T(8,128)} %concatenate.31.tab_ref, bf16[2,256,256]{2,1,0:T(8,128)(2,1)} %maximum_bitcast_fusion.q_ref, bf16[256,256]{1,0:T(8,128)(2,1)} %get-tuple-element.20.ku_ref, ...), custom_call_target="tpu_custom_call" | custom-call | tf_op jit(solution)/shard_map/pallas_call | solution.py:374
  72.9 78.1 %shard_map.173 = f32[64,2048]{1,0:T(8,128)} custom-call(bf16[64,2048]{1,0:T(8,128)(2,1)} %get-tuple-element.8.norm_ref, bf16[64,2048]{1,0:T(8,128)(2,1)} %get-tuple-element.9.hid_ref, f32[8,8,128]{2,1,0:T(8,128)} %get-tuple-element.10.tab_ref, bf16[2048,384]{1,0:T(8,128)(2,1)} %bitcast.21, bf16[2048,384]{1,0:T(8,128)(2,1)} %bitcast.22, ...), custom_call_target="tpu_custom_call" | custom-call | tf_op jit(solution)/shard_map/pallas_call | solution.py:630
  151.0 1.8 %convert_element_type.51 = bf16[64,2048]{1,0:T(8,128)(2,1)} convert(f32[64,2048]{1,0:T(8,128)} %shard_map.173) | non-fusion elementwise | flops 131072 | bytes 786432 | tf_op jit(solution)/shard_map/convert_element_type | solution.py:725
  (21 shorter events, 0.1 us)
Async XLA Ops:
  0.0 1.9 %copy-start.1 = (bf16[256,256]{1,0:T(8,128)(2,1)S(1)}, bf16[256,256]{1,0:T(8,128)(2,1)}, u32[]{:S(2)}) copy-start(bf16[256,256]{1,0:T(8,128)(2,1)} %param.18) | copy-start | bytes 393220
  1.5 1.6 %copy-start.2 = (bf16[256,64]{0,1:T(8,128)(2,1)S(1)}, bf16[256,64]{0,1:T(8,128)(2,1)}, u32[]{:S(2)}) copy-start(bf16[256,64]{0,1:T(8,128)(2,1)} %param.21) | copy-start | bytes 98308
  1.8 2.2 %copy-start = (bf16[256,256]{1,0:T(8,128)(2,1)S(1)}, bf16[256,256]{1,0:T(8,128)(2,1)}, u32[]{:S(2)}) copy-start(bf16[256,256]{1,0:T(8,128)(2,1)} %param.20) | copy-start | bytes 393220
  1.8 2.3 %copy-start.6 = (bf16[256]{0:T(256)(128)(2,1)S(1)}, bf16[256]{0:T(256)(128)(2,1)}, u32[]{:S(2)}) copy-start(bf16[256]{0:T(256)(128)(2,1)} %param.22) | copy-start | bytes 1540
  2.0 4.6 %copy-start.3 = (s32[64,4]{0,1:T(4,128)S(1)}, s32[64,4]{0,1:T(4,128)}, u32[]{:S(2)}) copy-start(s32[64,4]{0,1:T(4,128)} %param.28) | copy-start | bytes 3076
  2.3 5.0 %copy-start.5 = (f32[64,4]{0,1:T(4,128)S(1)}, f32[64,4]{0,1:T(4,128)}, u32[]{:S(2)}) copy-start(f32[64,4]{0,1:T(4,128)} %param.29) | copy-start | bytes 3076
  2.3 5.6 %copy-start.4 = (bf16[2048]{0:T(1024)(128)(2,1)S(1)}, bf16[2048]{0:T(1024)(128)(2,1)}, u32[]{:S(2)}) copy-start(bf16[2048]{0:T(1024)(128)(2,1)} %param.27) | copy-start | bytes 12292

commit v6 on v5

--- a/solution.py
+++ b/solution.py
@@ -18,30 +18,6 @@
 norm_eps = 1e-06
 
 
-def scale_rows(values, gain_vec):
-    as_float = values.astype(jnp.float32)
-    factor = lax.rsqrt(jnp.mean(as_float * as_float, axis=-1, keepdims=True) + norm_eps)
-    return (as_float * factor * gain_vec.astype(jnp.float32)).astype(jnp.bfloat16)
-
-
-def rotate(values, positions):
-    half_dim = values.shape[-1] // 2
-    frequency = rope_base ** (-jnp.arange(half_dim, dtype=jnp.float32) / half_dim)
-    angles = positions.astype(jnp.float32)[:, None, None] * frequency
-    cosine = jnp.cos(angles)
-    sine_part = jnp.sin(angles)
-    as_float = values.astype(jnp.float32)
-    first_half = as_float[..., :half_dim]
-    second_half = as_float[..., half_dim:]
-    return jnp.concatenate(
-        [
-            first_half * cosine - second_half * sine_part,
-            first_half * sine_part + second_half * cosine,
-        ],
-        axis=-1,
-    ).astype(jnp.bfloat16)
-
-
 LOG2E = 1.4426950408889634
 MESH_ID = pl.DeviceIdType.MESH
 SUBS = 4
@@ -54,18 +30,14 @@
     return lax.rem(value + size, size)
 
 
-def greet(partners):
-    barrier = pltpu.get_barrier_semaphore()
-    for dev in partners:
-        pl.semaphore_signal(barrier, inc=1, device_id=dev, device_id_type=MESH_ID)
-    pl.semaphore_wait(barrier, len(partners))
-
-
 def gather_attend_kernel(
-    pay_ref, tab_ref, q_ref, ku_ref, vu_ref, op_ref, res_ref, fg_ref, hid_ref, norm_ref, tabs_ref,
-    G, T, m_ref, l_ref, acc_ref, W, HS, HX,
+    lat_ref, kr_ref, qn_ref, qr_ref, cos_ref, sin_ref, lg_ref, tab_ref, res_ref, fg_ref,
+    ku_h, vu_h, op_ref, wg_h, wu_h, wd_h, sg_h, su_h, sd_h, out_ref,
+    G, T, m_ref, l_ref, acc_ref, W, HS, HX, q_ref, ku_ref, vu_ref,
+    HID, ACC, COL, OUT, ARR, EO, RET, PART, RD, RU, wg, wu, wd, sg, su, sd,
     recv, trecv, zsend, tsend, xsend, fsend, ysend, csend, lsem,
-    wrecv, wsend, wfsend, wcsend, hrecv, hsend,
+    wrecv, wsend, wfsend, wcsend, hrecv, hsend, usem, wsem,
+    ezrecv, ezsend, arecv, asend, rrecv, rsend, drecv, dsend, elsem,
 ):
     z, x, c, y = (lax.axis_index(n) for n in ("z", "x", "core", "y"))
     hm = lax.rem(y, 2)
@@ -76,7 +48,23 @@
     mate = {"core": 1 - c}
     xs = {0: x, -1: ring(x - 1, NX), 1: ring(x + 1, NX), 2: ring(x + 2, NX)}
     ZZ = [ring(z + off, NZ) for off in OFFS]
-    greet([up, down, right, left, above, below, mate])
+    me = x * NC + c
+    peers = []
+    for q in range(1, 8):
+        p = ring(me + q, 8)
+        peers.append((p, {"x": p // NC, "core": lax.rem(p, NC)}))
+    partners = [up, down, above, below] + [dev for _, dev in peers]
+    barrier = pltpu.get_barrier_semaphore()
+    for dev in partners:
+        pl.semaphore_signal(barrier, inc=1, device_id=dev, device_id_type=MESH_ID)
+
+    mine_cols = pl.ds(pl.multiple_of(y * 256, 256), 256)
+    ups = [
+        pltpu.make_async_copy(src.at[:, mine_cols], dst, usem.at[n])
+        for n, (src, dst) in enumerate(((ku_h, ku_ref), (vu_h, vu_ref)))
+    ]
+    for copy in ups:
+        copy.start()
 
     def piece(zz, xx, h, sem, dev):
         slot = G.at[c, zz, xx, h]
@@ -204,16 +192,54 @@
     ]
     for copy in own_proj:
         copy.start()
-    own = pltpu.make_async_copy(pay_ref, G.at[c, z, x], lsem.at[0])
-    own_table = pltpu.make_async_copy(tab_ref, T.at[z], lsem.at[1])
-    own.start()
-    own_table.start()
-    own.wait()
-    own_table.wait()
-
-    m_ref[...] = jnp.full(m_ref.shape, -1e30, jnp.float32)
-    l_ref[...] = jnp.zeros(l_ref.shape, jnp.float32)
-    acc_ref[...] = jnp.zeros(acc_ref.shape, jnp.float32)
+    lane = lax.broadcasted_iota(jnp.int32, (1, 128), 1)
+
+    def turn(values):
+        ahead, behind = pltpu.roll(values, 96, 1), pltpu.roll(values, 32, 1)
+        other = jnp.where(lane % 64 < 32, ahead, behind)
+        return values * cos_ref[...] + other * sin_ref[...]
+
+    lat = lat_ref[...].astype(jnp.float32)
+    factor = lax.rsqrt(jnp.sum(lat * lat, axis=1, keepdims=True) * (1.0 / 256) + norm_eps)
+    lat = (lat * factor * lg_ref[...].astype(jnp.float32)).astype(jnp.bfloat16)
+    keys_rope = kr_ref[...].astype(jnp.float32)
+    keys_rope = turn(jnp.concatenate([keys_rope, keys_rope], axis=1))
+    for h in range(2):
+        G[c, z, x, h, 0:128, :] = lat[h * 128 : (h + 1) * 128]
+        for n in range(2):
+            lo = h * 128 + n * 64
+            both = jnp.where(lane < 64, keys_rope[lo : lo + 32], keys_rope[lo + 32 : lo + 64])
+            G[c, z, x, h, 128:HALF, n * 128 : (n + 1) * 128] = both.astype(jnp.bfloat16)
+    T[z] = tab_ref[...]
+    pl.semaphore_wait(barrier, len(partners))
+
+    weights = [
+        pltpu.make_async_copy(src, dst, wsem.at[n])
+        for n, (src, dst) in enumerate(
+            ((wg_h, wg), (wu_h, wu), (wd_h, wd), (sg_h, sg), (su_h, su), (sd_h, sd))
+        )
+    ]
+
+    turned = turn(qr_ref[...].astype(jnp.float32)).astype(jnp.bfloat16)
+
+    def prepare():
+        for h in range(2):
+            q_ref[h] = jnp.concatenate(
+                [
+                    qn_ref[:, h * NOPE : (h + 1) * NOPE],
+                    turned[:, h * ROPE : (h + 1) * ROPE],
+                    jnp.zeros((ROWS, 64), jnp.bfloat16),
+                ],
+                axis=1,
+            )
+        for copy in ups:
+            copy.wait()
+        for w in weights:
+            w.start()
+        m_ref[...] = jnp.full(m_ref.shape, -1e30, jnp.float32)
+        l_ref[...] = jnp.zeros(l_ref.shape, jnp.float32)
+        acc_ref[...] = jnp.zeros(acc_ref.shape, jnp.float32)
+
     scale = LOG2E / math.sqrt(NOPE + ROPE)
     keys = 512
 
@@ -268,6 +294,8 @@
             def _():
                 if k < 8:
                     ev_z(k)
+                if k == 0:
+                    prepare()
                 if 0 <= k - 1 < 8:
                     ev_x1(k - 1)
                 if 0 <= k - 2 < 8:
@@ -328,7 +356,6 @@
     for yy in (y2, ya, yb):
         heads_to(yy).start()
     HX[y] = HS[y]
-    tabs_ref[...] = T[...]
     for yy in (yb, ya, y2):
         for r in range(8):
             proj_in(yy, 1 - c, r)
@@ -346,13 +373,20 @@
             rows = jnp.dot(HX[q], weight, preferred_element_type=jnp.float32)
             total = total + rows.astype(jnp.bfloat16).astype(jnp.float32)
         one = (res_ref[:, lanes].astype(jnp.float32) + total).astype(jnp.bfloat16)
-        hid_ref[:, lanes] = one
+        HID[:, lanes] = one
         one = one.astype(jnp.float32)
         squares = squares + jnp.sum(one * one, axis=1, keepdims=True)
     factor = lax.rsqrt(squares * (1.0 / 2048) + norm_eps)
-    norm_ref[...] = (
-        hid_ref[...].astype(jnp.float32) * factor * fg_ref[...].astype(jnp.float32)
-    ).astype(jnp.bfloat16)
+    for b in range(SUBS):
+        lanes = slice(b * WIDE, (b + 1) * WIDE)
+        COL[0, b] = (
+            HID[:, lanes].astype(jnp.float32) * factor * fg_ref[:, lanes].astype(jnp.float32)
+        ).astype(jnp.bfloat16)
+    experts_part(
+        z, x, c, y, up, down, peers, weights, out_ref,
+        T, HID, ACC, COL, OUT, ARR, EO, RET, PART, RD, RU, wg, wu, wd, sg, su, sd,
+        ezrecv, ezsend, arecv, asend, rrecv, rsend, drecv, dsend, elsem,
+    )
     for yy in (y2, ya, yb):
         heads_to(yy).wait_send()
     pltpu.make_async_remote_copy(
@@ -368,76 +402,64 @@
     ).wait_send()
 
 
-def gather_attend(payload, tables, q_cat, key_local, value_local, out_proj, residual, gain):
+def layer(small, large):
     vmem = pl.BlockSpec(memory_space=pltpu.VMEM)
     hbm = pl.BlockSpec(memory_space=pl.ANY)
+    bf, f32, dma = jnp.bfloat16, jnp.float32, pltpu.SemaphoreType.DMA
+    d, f = large[3].shape
+    shapes = [
+        ((2, NZ, NX, 2, HALF, 256), bf),
+        ((NZ, 8, 128), f32),
+        ((2, ROWS, 128), f32),
+        ((2, ROWS, 128), f32),
+        ((2, ROWS, 128), f32),
+        ((NY, 2, 8, 32, 1024), bf),
+        ((NY, 64, 256), bf),
+        ((NY, 64, 256), bf),
+        ((2, ROWS, 256), bf),
+        ((256, 256), bf),
+        ((256, 256), bf),
+        ((64, d), bf),
+        ((64, d), f32),
+        ((8, SUBS, 64, WIDE), bf),
+        ((8, 8, CAP, d), bf),
+        ((8, 8, CAP, d), bf),
+        ((8, 8, CAP, d), bf),
+        ((8, 8, CAP, d), bf),
+        ((8, SUBS, 64, WIDE), bf),
+        ((4, SUBS, 64, WIDE), bf),
+        ((4, SUBS, 64, WIDE), bf),
+        ((d, f), bf),
+        ((d, f), bf),
+        ((f, d), bf),
+        ((d, f), bf),
+        ((d, f), bf),
+        ((f, d), bf),
+    ]
+    sems = [
+        (2, NZ, NX, 2), (NZ,), (2, 4, 2), (2, 4), (8, 2), (8,), (8, 3), (), (4,),
+        (NY, 2, 8), (2, 8), (8,), (), (NY,), (NY,), (2,), (6,),
+        (8, SUBS), (8, SUBS), (8,), (8,), (8,), (8,), (2, 4, SUBS), (2, 4, SUBS), (3,),
+    ]
     return pl.pallas_call(
         gather_attend_kernel,
-        out_shape=(
-            jax.ShapeDtypeStruct((64, 2048), jnp.bfloat16),
-            jax.ShapeDtypeStruct((64, 2048), jnp.bfloat16),
-            jax.ShapeDtypeStruct((NZ, 8, 128), jnp.float32),
-        ),
-        in_specs=[vmem] * 5 + [hbm, vmem, vmem],
-        out_specs=(vmem, vmem, vmem),
-        scratch_shapes=[
-            pltpu.VMEM((2, NZ, NX, 2, HALF, 256), jnp.bfloat16),
-            pltpu.VMEM((NZ, 8, 128), jnp.float32),
-            pltpu.VMEM((2, ROWS, 128), jnp.float32),
-            pltpu.VMEM((2, ROWS, 128), jnp.float32),
-            pltpu.VMEM((2, ROWS, 128), jnp.float32),
-            pltpu.VMEM((NY, 2, 8, 32, 1024), jnp.bfloat16),
-            pltpu.VMEM((NY, 64, 256), jnp.bfloat16),
-            pltpu.VMEM((NY, 64, 256), jnp.bfloat16),
-            pltpu.SemaphoreType.DMA((2, NZ, NX, 2)),
-            pltpu.SemaphoreType.DMA((NZ,)),
-            pltpu.SemaphoreType.DMA((2, 4, 2)),
-            pltpu.SemaphoreType.DMA((2, 4)),
-            pltpu.SemaphoreType.DMA((8, 2)),
-            pltpu.SemaphoreType.DMA((8,)),
-            pltpu.SemaphoreType.DMA((8, 3)),
-            pltpu.SemaphoreType.DMA,
-            pltpu.SemaphoreType.DMA((4,)),
-            pltpu.SemaphoreType.DMA((NY, 2, 8)),
-            pltpu.SemaphoreType.DMA((2, 8)),
-            pltpu.SemaphoreType.DMA((8,)),
-            pltpu.SemaphoreType.DMA,
-            pltpu.SemaphoreType.DMA((NY,)),
-            pltpu.SemaphoreType.DMA((NY,)),
-        ],
+        out_shape=jax.ShapeDtypeStruct((64, 2048), jnp.bfloat16),
+        in_specs=[vmem] * len(small) + [hbm] * len(large),
+        out_specs=vmem,
+        scratch_shapes=[pltpu.VMEM(*shape) for shape in shapes]
+        + [dma(shape) if shape else dma for shape in sems],
         compiler_params=pltpu.CompilerParams(
             collective_id=0, has_side_effects=True, vmem_limit_bytes=63 * 1024 * 1024
         ),
-    )(
-        payload, tables, q_cat, key_local, value_local, out_proj.reshape(8, 32, 2048), residual,
-        gain.reshape(1, 2048),
-    )
-
-
-def moe_kernel(
-    norm_ref, hid_ref, tab_ref, wg_h, wu_h, wd_h, sg_h, su_h, sd_h, out_ref,
-    COL, OUT, ARR, EO, RET, PART, RD, RU, wg, wu, wd, sg, su, sd,
-    zrecv, zsend, arecv, asend, rrecv, rsend, drecv, dsend, lsem, wsem,
+    )(*small, *large)
+
+
+def experts_part(
+    z, x, c, y, up, down, peers, weights, out_ref,
+    T, HID, ACC, COL, OUT, ARR, EO, RET, PART, RD, RU, wg, wu, wd, sg, su, sd,
+    zrecv, zsend, arecv, asend, rrecv, rsend, drecv, dsend, lsem,
 ):
-    z, x, c, y = (lax.axis_index(n) for n in ("z", "x", "core", "y"))
     me = x * NC + c
-    up, down = {"z": ring(z + 1, NZ)}, {"z": ring(z - 1, NZ)}
-    peers = []
-    for q in range(1, 8):
-        p = ring(me + q, 8)
-        peers.append((p, {"x": p // NC, "core": lax.rem(p, NC)}))
-
-    weights = [
-        pltpu.make_async_copy(src, dst, wsem.at[n])
-        for n, (src, dst) in enumerate(
-            ((wg_h, wg), (wu_h, wu), (wd_h, wd), (sg_h, sg), (su_h, su), (sd_h, sd))
-        )
-    ]
-    for b in range(SUBS):
-        COL[0, b] = norm_ref[:, b * WIDE : (b + 1) * WIDE]
-    for w in weights:
-        w.start()
-    greet([up, down] + [dev for _, dev in peers])
 
     at = {off: i for i, off in enumerate(OFFS)}
 
@@ -491,7 +513,7 @@
     slots = lax.broadcasted_iota(jnp.int32, (64, 64), 0).astype(jnp.float32)
 
     def matches(i):
-        tab = tab_ref[ring(z + OFFS[i], NZ)]
+        tab = T[ring(z + OFFS[i], NZ)]
         base = (z * 64).astype(jnp.float32)
         return [(tab[k : k + 1, 0:64] - base) == slots for k in range(4)], tab
 
@@ -547,8 +569,8 @@
         for w in weights[3:]:
             w.wait()
         rows = jnp.concatenate([COL[0, b] for b in range(SUBS)], axis=1)
-        out_ref[...] = (
-            hid_ref[...].astype(jnp.float32)
+        ACC[...] = (
+            HID[...].astype(jnp.float32)
             + gated(rows, sg, su, sd).astype(jnp.bfloat16).astype(jnp.float32)
         )
 
@@ -613,55 +635,14 @@
             + RD[0, n].astype(jnp.float32)
             + RU[0, n].astype(jnp.float32)
         )
-        out_ref[:, lanes] = out_ref[:, lanes] + routed.astype(jnp.bfloat16).astype(jnp.float32)
+        total = ACC[:, lanes] + routed.astype(jnp.bfloat16).astype(jnp.float32)
+        out_ref[:, lanes] = total.astype(jnp.bfloat16)
 
     for copy in sends:
         copy.wait_send()
     for i in range(8):
         pieces_sent(i, OUT, asend)
         pieces_sent(i, EO, rsend)
-
-
-def experts_layer(normed, hidden, tables, wg, wu, wd, sg, su, sd):
-    vmem = pl.BlockSpec(memory_space=pltpu.VMEM)
-    hbm = pl.BlockSpec(memory_space=pl.ANY)
-    d, f = wg.shape
-    bf = jnp.bfloat16
-    return pl.pallas_call(
-        moe_kernel,
-        out_shape=jax.ShapeDtypeStruct((64, d), jnp.float32),
-        in_specs=[vmem] * 3 + [hbm] * 6,
-        out_specs=vmem,
-        scratch_shapes=[
-            pltpu.VMEM((8, SUBS, 64, WIDE), bf),
-            pltpu.VMEM((8, 8, CAP, d), bf),
-            pltpu.VMEM((8, 8, CAP, d), bf),
-            pltpu.VMEM((8, 8, CAP, d), bf),
-            pltpu.VMEM((8, 8, CAP, d), bf),
-            pltpu.VMEM((8, SUBS, 64, WIDE), bf),
-            pltpu.VMEM((4, SUBS, 64, WIDE), bf),
-            pltpu.VMEM((4, SUBS, 64, WIDE), bf),
-            pltpu.VMEM((d, f), bf),
-            pltpu.VMEM((d, f), bf),
-            pltpu.VMEM((f, d), bf),
-            pltpu.VMEM((d, f), bf),
-            pltpu.VMEM((d, f), bf),
-            pltpu.VMEM((f, d), bf),
-            pltpu.SemaphoreType.DMA((8, SUBS)),
-            pltpu.SemaphoreType.DMA((8, SUBS)),
-            pltpu.SemaphoreType.DMA((8,)),
-            pltpu.SemaphoreType.DMA((8,)),
-            pltpu.SemaphoreType.DMA((8,)),
-            pltpu.SemaphoreType.DMA((8,)),
-            pltpu.SemaphoreType.DMA((2, 4, SUBS)),
-            pltpu.SemaphoreType.DMA((2, 4, SUBS)),
-            pltpu.SemaphoreType.DMA((3,)),
-            pltpu.SemaphoreType.DMA((6,)),
-        ],
-        compiler_params=pltpu.CompilerParams(
-            collective_id=1, has_side_effects=True, vmem_limit_bytes=63 * 1024 * 1024
-        ),
-    )(normed, hidden, tables, wg, wu, wd, sg, su, sd)
 
 
 def body(
@@ -688,23 +669,11 @@
     q_sp = (z * NX + x) * NC + core
     first_row = q_sp * ROWS
     positions = first_row + jnp.arange(ROWS, dtype=jnp.int32)
-
-    normed_latent = scale_rows(latent, latent_gain)
-    rot_key = rotate(key_rope[:, None, :], positions)[:, 0, :]
-    packed = rot_key.reshape(2, 4, 32, ROPE).transpose(0, 2, 1, 3).reshape(2, 32, 256)
-    payload = jnp.concatenate([normed_latent.reshape(2, 128, 256), packed], axis=1)
-
-    key_local = lax.dynamic_slice_in_dim(key_up, y * 256, 256, 1)
-    value_local = lax.dynamic_slice_in_dim(value_up, y * 256, 256, 1)
-    rot_query = rotate(query_rope.reshape(ROWS, 2, ROPE), positions)
-    q_cat = jnp.concatenate(
-        [
-            query_nope.reshape(ROWS, 2, NOPE),
-            rot_query,
-            jnp.zeros((ROWS, 2, 64), jnp.bfloat16),
-        ],
-        axis=-1,
-    ).transpose(1, 0, 2)
+    half_dim = ROPE // 2
+    frequency = rope_base ** (-jnp.arange(half_dim, dtype=jnp.float32) / half_dim)
+    angles = positions.astype(jnp.float32)[:, None] * jnp.concatenate([frequency] * 4)[None, :]
+    sign = jnp.where(jnp.arange(128) % ROPE < half_dim, -1.0, 1.0)
+    cosine, sine_part = jnp.cos(angles), jnp.sin(angles) * sign[None, :]
 
     flat_ids = expert_ids.reshape(-1)
     onehot = (flat_ids[:, None] == jnp.arange(64, dtype=jnp.int32)[None, :]).astype(jnp.float32)
@@ -715,14 +684,15 @@
     rank = jnp.sum(before * onehot, axis=1).reshape(64, 4)
     tables = jnp.concatenate([expert_ids.astype(jnp.float32) * CAP + rank, route_weights], axis=1)
     tables = jnp.concatenate([tables.T, jnp.zeros((8, 64), jnp.float32)], axis=1)
-    hidden_one, normed, gathered = gather_attend(
-        payload, tables, q_cat, key_local, value_local, out_proj, residual, ffn_gain
+    small = (
+        latent, key_rope, query_nope, query_rope, cosine, sine_part, latent_gain.reshape(1, 256),
+        tables, residual, ffn_gain.reshape(1, 2048),
     )
-    summed = experts_layer(
-        normed, hidden_one, gathered, expert_gate[0], expert_up[0], expert_down[0],
-        shared_gate, shared_up, shared_down,
+    large = (
+        key_up, value_up, out_proj.reshape(8, 32, 2048), expert_gate[0], expert_up[0],
+        expert_down[0], shared_gate, shared_up, shared_down,
     )
-    return summed.astype(jnp.bfloat16)
+    return layer(small, large)
 
 
 def solution(mesh):

time: 153 us -> 148 us (0.967)
  Pallas kernels: 143 us -> 138 us
  local copies, waits for them, and re-layouts: 5.36 us -> 7.3 us
  other arithmetic: 4.44 us -> 2.72 us
    pallas_call x2 -> x1, Pallas kernels: 143 us -> 138 us  [layer(): pl.pallas_call(gather_attend_kernel, out_shape=jax.ShapeDtypeStruct((64,...]
    unnamed x19 -> x3, local copies, waits for them, and re-layouts: 1.42 us -> 3.92 us
    convert_element_type x5 -> x1, other arithmetic: 1.89 us -> 0.01 us  [body(): positions.astype(jnp.float32)[:, None]]
    reshape x3 -> x2, local copies, waits for them, and re-layouts: 0.83 us -> 2.51 us  [the longest x1 1.28 us: body(): ffn_gain.reshape(1, 2048)]
    dynamic_slice x1 -> x0, local copies, waits for them, and re-layouts: 1.68 us -> none  [body(): value_local = lax.dynamic_slice_in_dim(value_up, y * 256, 256, 1)]
where the time goes in v6:
time: 148 us
  Pallas kernels  138 us (93%)
  local copies, waits for them, and re-layouts  7.3 us (5%)
  other arithmetic  2.72 us (2%)
    pallas_call x1, Pallas kernels, layer(): pl.pallas_call(gather_attend_kernel, out_shape=jax.ShapeDtypeStruct((64,...  138 us
    unnamed x3, local copies, waits for them, and re-layouts  3.92 us

profile of v6, /device:TPU:1, one launch (start us, length us, event | category | flops | bytes accessed | tf_op | source)
XLA Modules:
  0.0 148.0 jit_solution(16856210948155955614)
XLA Ops:
  0.0 0.1 compare_select_fusion
  0.1 1.2 reshape.30.lg_ref
  1.3 1.3 reshape.32.fg_ref
  2.6 0.8 copy.20
  3.4 0.1 eq.17
  3.5 0.2 fusion
  3.7 0.1 reshape.31
  3.8 0.1 copy.21
  3.9 0.7 multiply_add_fusion
  4.6 0.7 maximum_bitcast_fusion
  5.3 0.6 concatenate.11.tab_ref
  5.9 1.5 copy.22.kr_ref
  7.3 1.2 fusion.1
  8.6 137.7 %shard_map.172 = bf16[64,2048]{1,0:T(8,128)(2,1)} custom-call(bf16[256,256]{1,0:T(8,128)(2,1)} %lat_ref.1, bf16[256,64]{1,0:T(8,128)(2,1)} %copy.22.kr_ref, bf16[256,256]{1,0:T(8,128)(2,1)} %qn_ref.1, bf16[256,128]{1,0:T(8,128)(2,1)} %qr_ref.1, f32[256,128]{1,0:T(8,128)} %get-tuple-element.6.cos_ref, f32[256,128]{1,0:T(8,128)} %get-tuple-element.5.sin_ref, ...), custom_call_target="tpu_custom_call" | custom-call | tf_op jit(solution)/shard_map/pallas_call | solution.py:444
  146.3 1.7 %copy.24 = bf16[64,2048]{1,0:T(8,128)(2,1)} copy(bf16[64,2048]{1,0:T(8,128)(2,1)} %shard_map.172) | data formatting | bytes 524288
  (2 shorter events, 0.0 us)

commit v7 on v6

--- a/solution.py
+++ b/solution.py
@@ -31,7 +31,7 @@
 
 
 def gather_attend_kernel(
-    lat_ref, kr_ref, qn_ref, qr_ref, cos_ref, sin_ref, lg_ref, tab_ref, res_ref, fg_ref,
+    lat_ref, kr_ref, qn_ref, qr_ref, cos_ref, sin_ref, lg_ref, ids_ref, rw_ref, res_ref, fg_ref,
     ku_h, vu_h, op_ref, wg_h, wu_h, wd_h, sg_h, su_h, sd_h, out_ref,
     G, T, m_ref, l_ref, acc_ref, W, HS, HX, q_ref, ku_ref, vu_ref,
     HID, ACC, COL, OUT, ARR, EO, RET, PART, RD, RU, wg, wu, wd, sg, su, sd,
@@ -201,8 +201,8 @@
 
     lat = lat_ref[...].astype(jnp.float32)
     factor = lax.rsqrt(jnp.sum(lat * lat, axis=1, keepdims=True) * (1.0 / 256) + norm_eps)
-    lat = (lat * factor * lg_ref[...].astype(jnp.float32)).astype(jnp.bfloat16)
-    keys_rope = kr_ref[...].astype(jnp.float32)
+    lat = (lat * factor * lg_ref[...].astype(jnp.float32).reshape(1, 256)).astype(jnp.bfloat16)
+    keys_rope = kr_ref[...].astype(jnp.float32).T
     keys_rope = turn(jnp.concatenate([keys_rope, keys_rope], axis=1))
     for h in range(2):
         G[c, z, x, h, 0:128, :] = lat[h * 128 : (h + 1) * 128]
@@ -210,7 +210,22 @@
             lo = h * 128 + n * 64
             both = jnp.where(lane < 64, keys_rope[lo : lo + 32], keys_rope[lo + 32 : lo + 64])
             G[c, z, x, h, 128:HALF, n * 128 : (n + 1) * 128] = both.astype(jnp.bfloat16)
-    T[z] = tab_ref[...]
+    ids = ids_ref[...].astype(jnp.float32)
+    expert = lax.broadcasted_iota(jnp.int32, (64, 64), 0).astype(jnp.float32)
+    named = [jnp.where(ids[k : k + 1] == expert, 1.0, 0.0) for k in range(4)]
+    earlier = jnp.where(
+        lax.broadcasted_iota(jnp.int32, (64, 64), 0) < lax.broadcasted_iota(jnp.int32, (64, 64), 1),
+        1.0,
+        0.0,
+    )
+    before = jnp.dot(
+        (named[0] + named[1] + named[2] + named[3]).astype(jnp.bfloat16),
+        earlier.astype(jnp.bfloat16),
+        preferred_element_type=jnp.float32,
+    )
+    rank = [jnp.sum(one * before, axis=0, keepdims=True) for one in named]
+    table_rows = jnp.concatenate([ids * CAP + jnp.concatenate(rank, axis=0), rw_ref[...]], axis=0)
+    T[z] = jnp.concatenate([table_rows, jnp.zeros((8, 64), jnp.float32)], axis=1)
     pl.semaphore_wait(barrier, len(partners))
 
     weights = [
@@ -377,10 +392,11 @@
         one = one.astype(jnp.float32)
         squares = squares + jnp.sum(one * one, axis=1, keepdims=True)
     factor = lax.rsqrt(squares * (1.0 / 2048) + norm_eps)
+    gain = fg_ref[...].astype(jnp.float32).reshape(1, 2048)
     for b in range(SUBS):
         lanes = slice(b * WIDE, (b + 1) * WIDE)
         COL[0, b] = (
-            HID[:, lanes].astype(jnp.float32) * factor * fg_ref[:, lanes].astype(jnp.float32)
+            HID[:, lanes].astype(jnp.float32) * factor * gain[:, lanes]
         ).astype(jnp.bfloat16)
     experts_part(
         z, x, c, y, up, down, peers, weights, out_ref,
@@ -675,18 +691,9 @@
     sign = jnp.where(jnp.arange(128) % ROPE < half_dim, -1.0, 1.0)
     cosine, sine_part = jnp.cos(angles), jnp.sin(angles) * sign[None, :]
 
-    flat_ids = expert_ids.reshape(-1)
-    onehot = (flat_ids[:, None] == jnp.arange(64, dtype=jnp.int32)[None, :]).astype(jnp.float32)
-    earlier = (
-        jnp.arange(256, dtype=jnp.int32)[None, :] < jnp.arange(256, dtype=jnp.int32)[:, None]
-    ).astype(jnp.float32)
-    before = jnp.dot(earlier, onehot)
-    rank = jnp.sum(before * onehot, axis=1).reshape(64, 4)
-    tables = jnp.concatenate([expert_ids.astype(jnp.float32) * CAP + rank, route_weights], axis=1)
-    tables = jnp.concatenate([tables.T, jnp.zeros((8, 64), jnp.float32)], axis=1)
     small = (
-        latent, key_rope, query_nope, query_rope, cosine, sine_part, latent_gain.reshape(1, 256),
-        tables, residual, ffn_gain.reshape(1, 2048),
+        latent, key_rope.T, query_nope, query_rope, cosine, sine_part, latent_gain,
+        expert_ids.T, route_weights.T, residual, ffn_gain,
     )
     large = (
         key_up, value_up, out_proj.reshape(8, 32, 2048), expert_gate[0], expert_up[0],

time: 148 us -> 141 us (0.953)
  local copies, waits for them, and re-layouts: 7.3 us -> 1.67 us
    reshape x4 -> x0, local copies, waits for them, and re-layouts: 2.69 us -> none  [the longest x1 1.28 us: body(): ffn_gain.reshape(1, 2048)]
    unnamed x3 -> x1, local copies, waits for them, and re-layouts: 3.92 us -> 1.67 us
where the time goes in v7:
time: 141 us
  Pallas kernels  138 us (98%)
  local copies, waits for them, and re-layouts  1.67 us (1%)
    pallas_call x1, Pallas kernels, layer(): pl.pallas_call(gather_attend_kernel, out_shape=jax.ShapeDtypeStruct((64,...  138 us

profile of v7, /device:TPU:1, one launch (start us, length us, event | category | flops | bytes accessed | tf_op | source)
XLA Modules:
  0.0 140.6 jit_solution(3238661485193289473)
XLA Ops:
  0.0 0.1 compare_select_fusion
  0.1 1.2 fusion
  1.3 137.5 %shard_map.172 = bf16[64,2048]{1,0:T(8,128)(2,1)} custom-call(bf16[256,256]{1,0:T(8,128)(2,1)} %lat_ref.1, bf16[64,256]{1,0:T(8,128)(2,1)} %bitcast.11, bf16[256,256]{1,0:T(8,128)(2,1)} %qn_ref.1, bf16[256,128]{1,0:T(8,128)(2,1)} %qr_ref.1, f32[256,128]{1,0:T(8,128)} %get-tuple-element.6.cos_ref, f32[256,128]{1,0:T(8,128)} %get-tuple-element.5.sin_ref, ...), custom_call_target="tpu_custom_call" | custom-call | tf_op jit(solution)/shard_map/pallas_call | solution.py:460
  138.9 1.7 %copy.20 = bf16[64,2048]{1,0:T(8,128)(2,1)} copy(bf16[64,2048]{1,0:T(8,128)(2,1)} %shard_map.172) | data formatting | bytes 524288
  (2 shorter events, 0.0 us)
